TPU v7x, 256 devices: a whole 4x4x8 slice. The times are simulated.
256 devices in a mesh: ep: 64 (over z, y, core), tp: 4 (over x).
Axes of the slice: x: 4, y: 4, z: 8, core: 2. Of those that a mesh axis runs over, the one named last changes fastest.
Arguments:
- outer_gate: bfloat16 [32768, 2048], P('ep', 'tp'), may hold values from -6 to 6
- inner_gate: bfloat16 [32768, 2048], P('ep', 'tp'), may hold values from -6 to 6
- conv_values: bfloat16 [32768, 2048], P('ep', 'tp'), may hold values from -6 to 6
- conv_taps: bfloat16 [3, 2048], P(None, 'tp'), may hold values from -3 to 3
- out_weight: bfloat16 [2048, 2048], P('tp'), may hold values from -0.125 to 0.125
- moe_input: bfloat16 [32768, 2048], P(('ep', 'tp')), may hold values from -6 to 6
- norm_gain: bfloat16 [2048], replicated, may hold values from 0.099609375 to 1.8984375
- gate_proj: bfloat16 [64, 2048, 1024], P('ep', None, 'tp'), may hold values from -0.125 to 0.125
- up_proj: bfloat16 [64, 2048, 1024], P('ep', None, 'tp'), may hold values from -0.125 to 0.125
- down_proj: bfloat16 [64, 1024, 2048], P('ep', 'tp'), may hold values from -0.1875 to 0.1875
- shared_gate: bfloat16 [2048, 1024], P(None, 'tp'), may hold values from -0.125 to 0.125
- shared_up: bfloat16 [2048, 1024], P(None, 'tp'), may hold values from -0.125 to 0.125
- shared_down: bfloat16 [1024, 2048], P('tp'), may hold values from -0.1875 to 0.1875
- routes: int32 [32768, 2], P('ep'), may hold values from 0 to 63, all different within a row; in each aligned block of 128 rows (0 to 127, 128 to 255, ...) at most 8 rows name the same one
- route_weight: float32 [32768, 2], P('ep'), may hold values from 0.3 to 1.5
Outputs:
- mixer_out: bfloat16 [32768, 2048], P(('ep', 'tp'))
- expert_mix: bfloat16 [32768, 2048], P(('ep', 'tp'))
Inputs may be any that keep to these rules, and one draw needn't show every extreme that they name: `routes`: each row names 2 different experts. In the 128 rows of one device no expert is named more than 8 times, and in every draw some expert is named exactly 8 times in one device's rows.
All inputs are finite; a program needn't handle non-finite values.
Results may differ from a plain program's by a relative error of at most 0.012.
Values may be sent and summed in bfloat16 or wider, within the bound.
A program may use at most 128 MiB of HBM per device.

v0:
```python
from functools import partial

import jax
import jax.numpy as jnp
from jax import lax
from jax.sharding import PartitionSpec as P

epsilon = 1e-06


def shifted(block, axis, distance):
    devices = range(lax.axis_size(axis))
    route = [(i - distance, i) for i in devices if i - distance in devices]
    return lax.ppermute(block, axis, route)


def from_everyone(array, axis):
    length = lax.axis_size(axis)
    return lax.all_to_all(
        jnp.broadcast_to(array[None], (length, *array.shape)), axis, 0, 0, tiled=True
    )


def joined_along(blocks, dim):
    shape = list(blocks.shape[1:])
    shape[dim] *= blocks.shape[0]
    return jnp.moveaxis(blocks, 0, dim).reshape(shape)


def collect(array, axis, dim):
    blocks = from_everyone(array, axis)
    return joined_along(blocks, dim)


def gather_turned(arrays, axis, dims):
    turned = [jnp.moveaxis(a, dim, 0) for a, dim in zip(arrays, dims)]
    both = jnp.concatenate([t.reshape(len(t), -1) for t in turned], axis=1)
    result, at, outs = (lax.all_gather(both, axis, axis=0, tiled=True), 0, [])
    for t, dim in zip(turned, dims):
        share = result[:, at : at + t[0].size].reshape(-1, *t.shape[1:])
        outs.append(jnp.moveaxis(share, 0, dim))
        at += t[0].size
    return tuple(outs)


def rms_norm(inputs, scales):
    values = inputs.astype(jnp.float32)
    square = jnp.mean(values * values, axis=-1, keepdims=True)
    return (values * lax.rsqrt(square + epsilon) * scales.astype(jnp.float32)).astype(jnp.bfloat16)


def swiglu(inputs, gate_w, up_w):
    gate_term = jnp.dot(inputs, gate_w, preferred_element_type=jnp.float32)
    upward = jnp.dot(inputs, up_w, preferred_element_type=jnp.float32)
    return (jax.nn.silu(gate_term) * upward).astype(jnp.bfloat16)


def slot_table(block_routes, experts, capacity):
    flat_ids = block_routes.reshape(-1)
    onehot = (flat_ids[:, None] == jnp.arange(experts, dtype=jnp.int32)[None, :]).astype(jnp.int32)
    earlier = jnp.cumsum(onehot, axis=0) - onehot
    slot_ids = jnp.sum(earlier * onehot, axis=1)
    targets = flat_ids * capacity + slot_ids
    owners = jnp.arange(flat_ids.shape[0], dtype=jnp.int32) // block_routes.shape[1]
    sources = jnp.zeros((experts * capacity,), jnp.int32).at[targets].set(owners)
    filled = jnp.zeros((experts * capacity,), jnp.bfloat16).at[targets].set(1.0)
    return (sources, filled, targets)


def send_own(normed, own_routes, table_maker, ep_count, capacity):
    sources, filled, own_targets = table_maker(own_routes)
    outgoing = (normed[sources] * filled[:, None]).reshape(ep_count, capacity, normed.shape[1])
    landed = lax.all_to_all(outgoing, "ep", split_axis=0, concat_axis=0, tiled=True)
    return (landed, own_targets)


def per_device(
    outer_gate,
    inner_gate,
    conv_values,
    conv_taps,
    out_weight,
    moe_input,
    norm_gain,
    gate_proj,
    up_proj,
    down_proj,
    shared_gate,
    shared_up,
    shared_down,
    routes,
    route_weight,
):
    tp_count = lax.axis_size("tp")
    ep_count = lax.axis_size("ep")
    my_slot = lax.axis_index("tp")
    group_len = inner_gate.shape[0]
    mix_rows = group_len // tp_count
    channels = inner_gate.shape[1]
    model_width = moe_input.shape[1]
    own_rows = moe_input.shape[0]
    top_count = routes.shape[1]
    capacity = 2 * own_rows * top_count // ep_count
    slot_rows = ep_count * capacity
    reach_rows = conv_taps.shape[0] - 1
    edge_rows = jnp.stack(
        (inner_gate[group_len - reach_rows :], conv_values[group_len - reach_rows :])
    )
    before = shifted(edge_rows, "ep", 1)
    full_gate = jnp.concatenate((before[0], inner_gate), axis=0).astype(jnp.float32)
    full_values = jnp.concatenate((before[1], conv_values), axis=0).astype(jnp.float32)
    product = full_gate * full_values
    tap_values = conv_taps.astype(jnp.float32)
    convolved = tap_values[0] * product[0:group_len]
    for offset in range(1, reach_rows + 1):
        convolved = convolved + tap_values[offset] * product[offset : offset + group_len]
    gate_rows = (outer_gate.astype(jnp.float32) * convolved).astype(jnp.bfloat16)
    gate_rows = gate_rows.reshape(tp_count, mix_rows, channels)
    normed = rms_norm(moe_input, norm_gain)
    group_normed = collect(normed, "tp", 0)
    group_split = group_normed.reshape(tp_count, own_rows, model_width)
    own_weights = lax.dynamic_slice_in_dim(route_weight, my_slot * own_rows, own_rows, 0)
    own_routes = lax.dynamic_slice_in_dim(routes, my_slot * own_rows, own_rows, 0)
    table_maker = partial(slot_table, experts=ep_count, capacity=capacity)
    local_routed = None
    landed, own_targets = send_own(normed, own_routes, table_maker, ep_count, capacity)
    gate_full, up_full, down_full = gather_turned((gate_proj, up_proj, down_proj), "tp", (2, 2, 1))
    hidden = swiglu(landed.reshape(slot_rows, model_width), gate_full[0], up_full[0])
    unit_block = hidden.shape[1] // tp_count
    local_routed = jnp.zeros((slot_rows, model_width), jnp.float32)
    for piece_idx in range(tp_count):
        partial_sum = jnp.dot(
            hidden[:, piece_idx * unit_block : (piece_idx + 1) * unit_block],
            down_full[0, piece_idx * unit_block : (piece_idx + 1) * unit_block],
            preferred_element_type=jnp.float32,
        ).astype(jnp.bfloat16)
        local_routed = local_routed + partial_sum.astype(jnp.float32)
    routed_rows = 0
    expert_block = routed_rows + own_rows
    joint_block = mix_rows + expert_block
    dev_count = joint_block * lax.axis_size("tp") // joint_block
    block_rows = gate_rows
    block_rows = block_rows.reshape(dev_count * mix_rows, channels)
    projected = jnp.dot(block_rows, out_weight, preferred_element_type=jnp.float32)
    shared_in = group_split
    shared_in = shared_in.reshape(dev_count * own_rows, model_width)
    shared_out = jnp.dot(
        swiglu(shared_in, shared_gate, shared_up), shared_down, preferred_element_type=jnp.float32
    )
    shared_out = shared_out.reshape(dev_count, own_rows, model_width)
    combined = jnp.concatenate(
        (projected.reshape(dev_count, mix_rows, model_width), shared_out), axis=1
    )
    summed = lax.psum_scatter(
        combined.reshape(dev_count * joint_block, model_width).astype(jnp.bfloat16),
        "tp",
        scatter_dimension=0,
        tiled=True,
    ).astype(jnp.float32)
    mixer_out = summed[:mix_rows].astype(jnp.bfloat16)
    expert_total = summed[mix_rows:]
    routed_back = local_routed.astype(jnp.bfloat16)
    routed_back = routed_back.reshape(ep_count, capacity, model_width)
    returned = lax.all_to_all(routed_back, "ep", split_axis=0, concat_axis=0, tiled=True).reshape(
        slot_rows, model_width
    )
    picked = returned[own_targets].reshape(own_rows, top_count, model_width).astype(jnp.float32)
    routed = jnp.sum(picked * own_weights[:, :, None], axis=1)
    expert_mix = (expert_total + routed).astype(jnp.bfloat16)
    return (mixer_out, expert_mix)


def solution(mesh):
    return jax.shard_map(
        per_device,
        mesh=mesh,
        in_specs=(
            P("ep", "tp"),
            P("ep", "tp"),
            P("ep", "tp"),
            P(None, "tp"),
            P("tp", None),
            P(("ep", "tp"), None),
            P(),
            P("ep", None, "tp"),
            P("ep", None, "tp"),
            P("ep", "tp", None),
            P(None, "tp"),
            P(None, "tp"),
            P("tp", None),
            P("ep", None),
            P("ep", None),
        ),
        out_specs=(P(("ep", "tp"), None), P(("ep", "tp"), None)),
        check_vma=False,
    )
```

profile of v0, /device:TPU:1, one launch (start us, length us, event | category | flops | bytes accessed | tf_op | source)
XLA Modules:
  0.0 244.6 jit_solution(8007941486165297258)
XLA Ops:
  7.2 1.6 copy.24
  8.9 2.3 copy.25
  11.1 3.0 %pad_maximum_fusion.1 = bf16[256,6144]{1,0:T(8,128)(2,1)} fusion(bf16[256,2048]{1,0:T(8,128)(2,1)} %bitcast.97, bf16[256,2048]{1,0:T(8,128)(2,1)} %bitcast.94, bf16[256,2048]{1,0:T(8,128)(2,1)S(1)} %bitcast.93), kind=kLoop, calls=%fused_computation.11 | loop fusion | flops 9437184 | bytes 6291456 | tf_op jit(solution)/shard_map/concatenate | solution.py:37
  15.6 1.6 broadcast_in_dim.8
  17.2 4.8 %all-to-all-start = ((bf16[4,128,2048]{2,1,0:T(8,128)(2,1)}), bf16[4,128,2048]{2,1,0:T(8,128)(2,1)}, u32[]{:S(2)}, u32[]{:S(2)}) async-start(bf16[4,128,2048]{2,1,0:T(8,128)(2,1)} %broadcast_in_dim.8), calls=%async_computation | async-start | bytes 4194304 | tf_op jit(solution)/shard_map/all_to_all | solution.py:19
  24.3 1.4 scatter_custom_fusion
  25.8 3.3 %gather_fusion = bf16[512,2048]{1,0:T(8,128)(2,1)} fusion(bf16[128,2048]{1,0:T(8,128)(2,1)S(1)} %fusion.10, s32[1024]{0:T(1024)S(1)} %pad_clamp_fusion.1), kind=kCustom, calls=%fused_computation | custom fusion | bytes 4196352 | tf_op jit(solution)/shard_map/gather | solution.py:72
  29.0 2.2 scatter_custom_fusion.1
  31.3 3.5 %bitcast_multiply_fusion = bf16[64,8,2048]{2,1,0:T(8,128)(2,1)} fusion(bf16[512,2048]{1,0:T(8,128)(2,1)} %gather_fusion, bf16[64,8]{1,0:T(8,128)(2,1)S(1)} %mul.134), kind=kLoop, calls=%fused_computation.21 | loop fusion | flops 1048576 | bytes 4195328 | tf_op jit(solution)/shard_map/mul | solution.py:72
  34.8 19.5 %all-to-all-done = bf16[4,128,2048]{2,1,0:T(8,128)(2,1)} async-done(((bf16[4,128,2048]{2,1,0:T(8,128)(2,1)}), bf16[4,128,2048]{2,1,0:T(8,128)(2,1)}, u32[]{:S(2)}, u32[]{:S(2)}) %all-to-all-start) | async-done | bytes 2097184 | tf_op jit(solution)/shard_map/all_to_all | solution.py:19
  54.3 21.7 %all-to-all-start.1 = ((bf16[64,8,2048]{2,1,0:T(8,128)(2,1)}), bf16[64,8,2048]{2,1,0:T(8,128)(2,1)}, u32[]{:S(2)}, u32[]{:S(2)}) async-start(bf16[64,8,2048]{2,1,0:T(8,128)(2,1)} %bitcast_multiply_fusion), calls=%async_computation.2 | async-start | bytes 4194304 | tf_op jit(solution)/shard_map/all_to_all | solution.py:73
  76.2 3.9 %collective-permute-start = (bf16[2,2,512]{2,1,0:T(2,128)(2,1)S(1)}, bf16[2,2,512]{2,1,0:T(2,128)(2,1)S(1)}, u32[]{:S(2)}, u32[]{:S(2)}) collective-permute-start(bf16[2,2,512]{2,1,0:T(2,128)(2,1)S(1)} %pad_maximum_fusion.2), channel_id=1, source_target_pairs={{0,4},{4,8},{8,12},{12,16},{16,20},{20,24},{24,28},{28,32},{32,36}... | collective-permute-start | bytes 12296 | tf_op jit(solution)/shard_map/ppermute | solution.py:14
  80.9 2.8 %convolution_convert_fusion.5 = bf16[512,2048]{1,0:T(8,128)(2,1)} fusion(bf16[512,2048]{1,0:T(8,128)(2,1)S(1)} %copy-done, f32[514,512]{1,0:T(8,128)S(1)} %convert_multiply_fusion.2, bf16[512,512]{1,0:T(8,128)(2,1)S(1)} %copy-done.12, f32[512]{0:T(512)S(1)} %bitcast.104, f32[512]{0:T(512)S(1)} %bitcast.103, f32[512]{0:T(512)S(1)} %bitcast.102), kind=kOutput, calls=%fused_computation.17 | convolution fusion | flops 1076887552 | bytes 7870464 | tf_op jit(solution)/shard_map/dot_general | solution.py:144
  83.6 3.2 %fusion.39 = f32[512,256]{1,0:T(8,128)} fusion(bf16[512,2048]{1,0:T(8,128)(2,1)} %bitcast.8, bf16[2048,256]{1,0:T(8,128)(2,1)S(1)} %copy-done.10), kind=kOutput, calls=%fused_computation.89 | convolution fusion | flops 536870912 | bytes 3670016 | tf_op jit(solution)/shard_map/dot_general | solution.py:53
  86.9 5.8 %convolution_convert_fusion.4 = bf16[512,2048]{1,0:T(8,128)(2,1)} fusion(bf16[256,2048]{1,0:T(8,128)(2,1)S(1)} %copy-done.11, bf16[512,2048]{1,0:T(8,128)(2,1)} %bitcast.8, bf16[2048,256]{1,0:T(8,128)(2,1)} %param.26, f32[512,256]{1,0:T(8,128)} %fusion.39), kind=kOutput, calls=%fused_computation.16 | convolution fusion | flops 1075576832 | bytes 6815744 | tf_op jit(solution)/shard_map/dot_general | solution.py:147
  92.7 4.2 %pad_maximum_fusion = bf16[4,256,2048]{2,1,0:T(8,128)(2,1)} fusion(bf16[4,128,2048]{2,1,0:T(8,128)(2,1)} %bitcast.96, bf16[4,128,2048]{2,1,0:T(8,128)(2,1)S(1)} %bitcast.95), kind=kLoop, calls=%fused_computation.9 | loop fusion | flops 8388608 | bytes 8388608 | tf_op jit(solution)/shard_map/concatenate | solution.py:151
  96.9 29.0 %all-to-all-done.1 = bf16[64,8,2048]{2,1,0:T(8,128)(2,1)} async-done(((bf16[64,8,2048]{2,1,0:T(8,128)(2,1)}), bf16[64,8,2048]{2,1,0:T(8,128)(2,1)}, u32[]{:S(2)}, u32[]{:S(2)}) %all-to-all-start.1) | async-done | bytes 2097184 | tf_op jit(solution)/shard_map/all_to_all | solution.py:73
  125.8 24.3 %all-gather.2.cloned.1.call-done = bf16[1024,6144]{1,0:T(8,128)(2,1)} async-done(((bf16[256,6144]{1,0:T(8,128)(2,1)}), bf16[1024,6144]{1,0:T(8,128)(2,1)}) %all-gather.2.cloned.1.call-update) | async-done | bytes 12582928 | tf_op jit(solution)/shard_map/all_gather | solution.py:38
  150.1 5.3 %fusion.1 = f32[512,1024]{1,0:T(8,128)S(1)} fusion(bf16[1024,6144]{1,0:T(8,128)(2,1)} %all-gather.2.cloned.1.call-done, bf16[64,8,2048]{2,1,0:T(8,128)(2,1)} %all-to-all-done.1), kind=kOutput, calls=%fused_computation.8 | convolution fusion | flops 2147483648 | bytes 8388608 | tf_op jit(solution)/shard_map/dot_general | solution.py:53
  155.5 1.1 copy-done.4
  157.1 4.1 %multiply_convert_fusion = bf16[512,1024]{1,0:T(8,128)(2,1)S(1)} fusion(f32[512,1024]{1,0:T(8,128)S(1)} %fusion.1, bf16[1024,6144]{1,0:T(8,128)(2,1)S(1)} %copy-done.4, bf16[64,8,2048]{2,1,0:T(8,128)(2,1)} %all-to-all-done.1), kind=kOutput, calls=%fused_computation.23 | convolution fusion | flops 2150629376 | bytes 9437184 | tf_op jit(solution)/shard_map/dot_general | solution.py:54
  161.3 0.7 convolution_convert_fusion.2
  162.0 0.7 convolution_convert_fusion.1
  163.4 2.6 %fusion.2 = bf16[64,8,2048]{2,1,0:T(8,128)(2,1)} fusion(bf16[512,2048]{1,0:T(8,128)(2,1)S(1)} %convolution_convert_fusion, bf16[512,2048]{1,0:T(8,128)(2,1)S(1)} %convolution_convert_fusion.1, bf16[512,2048]{1,0:T(8,128)(2,1)S(1)} %convolution_convert_fusion.2, bf16[1,1024,2048]{2,1,0:T(8,128)(2,1)S(1)} %slice_bitcast_fusion, ...), kind=kOutput, calls=%fused_computation.18 | convolution fusion | flops 546308096 | bytes 9699328 | tf_op jit(solution)/shard_map/dot_general | solution.py:132
  166.1 12.4 %all-to-all-start.2 = ((bf16[64,8,2048]{2,1,0:T(8,128)(2,1)}), bf16[64,8,2048]{2,1,0:T(8,128)(2,1)S(1)}, u32[]{:S(2)}, u32[]{:S(2)}) async-start(bf16[64,8,2048]{2,1,0:T(8,128)(2,1)} %fusion.2), calls=%async_computation.3 | async-start | bytes 4194304 | tf_op jit(solution)/shard_map/all_to_all | solution.py:164
  179.3 24.2 %reduce-scatter.2.cloned.1.call-done = bf16[256,2048]{1,0:T(8,128)(2,1)} async-done(((bf16[1024,2048]{1,0:T(8,128)(2,1)}), bf16[256,2048]{1,0:T(8,128)(2,1)}) %reduce-scatter.2.cloned.1.call-update) | async-done | bytes 1048592 | tf_op jit(solution)/shard_map/reduce_scatter | solution.py:154
  203.5 1.9 slice.117
  205.4 22.8 %all-to-all-done.2 = bf16[64,8,2048]{2,1,0:T(8,128)(2,1)S(1)} async-done(((bf16[64,8,2048]{2,1,0:T(8,128)(2,1)}), bf16[64,8,2048]{2,1,0:T(8,128)(2,1)S(1)}, u32[]{:S(2)}, u32[]{:S(2)}) %all-to-all-start.2) | async-done | bytes 2097184 | tf_op jit(solution)/shard_map/all_to_all | solution.py:164
  228.2 1.4 gather_fusion.1
  229.6 2.4 reshape.113
  231.9 4.9 %multiply_reduce_fusion = f32[128,2048]{1,0:T(8,128)S(1)} fusion(f32[128,2,2048]{2,1,0:T(2,128)} %reshape.113, f32[128,2]{1,0:T(8,128)S(1)} %copy.26), kind=kLoop, calls=%fused_computation.22 | loop fusion | flops 786432 | bytes 3146752 | tf_op jit(solution)/shard_map/reduce_sum | solution.py:168
  236.9 0.9 add_convert_fusion.1
  (62 shorter events, 6.9 us)
Async XLA Ops:
  7.2 73.7 %copy-start = (bf16[512,2048]{1,0:T(8,128)(2,1)S(1)}, bf16[512,2048]{1,0:T(8,128)(2,1)}, u32[]{:S(2)}) copy-start(bf16[512,2048]{1,0:T(8,128)(2,1)} %param.19) | copy-start | bytes 6291460
  7.2 143.0 %all-gather.2.cloned.1.call-start = ((), (), s32[]{:S(2)}) async-start(), calls=%async_computation.5 | async-start | bytes 15728640 | tf_op jit(solution)/shard_map/all_gather | solution.py:38
  14.1 0.7 copy-start.9
  14.1 1.1 copy-start.2
  17.2 37.2 %all-to-all-start = ((bf16[4,128,2048]{2,1,0:T(8,128)(2,1)}), bf16[4,128,2048]{2,1,0:T(8,128)(2,1)}, u32[]{:S(2)}, u32[]{:S(2)}) async-start(bf16[4,128,2048]{2,1,0:T(8,128)(2,1)} %broadcast_in_dim.8), calls=%async_computation | async-start | bytes 4194304 | tf_op jit(solution)/shard_map/all_to_all | solution.py:19
  34.8 41.3 %copy-start.6 = (bf16[512,512]{1,0:T(8,128)(2,1)S(1)}, bf16[512,512]{1,0:T(8,128)(2,1)}, u32[]{:S(2)}) copy-start(bf16[512,512]{1,0:T(8,128)(2,1)} %param.16) | copy-start | bytes 1572868
  34.8 41.3 %copy-start.7 = (bf16[512,512]{1,0:T(8,128)(2,1)S(1)}, bf16[512,512]{1,0:T(8,128)(2,1)}, u32[]{:S(2)}) copy-start(bf16[512,512]{1,0:T(8,128)(2,1)} %param.17) | copy-start | bytes 1572868
  34.8 45.2 %copy-start.8 = (bf16[3,512]{1,0:T(4,128)(2,1)S(1)}, bf16[3,512]{1,0:T(4,128)(2,1)}, u32[]{:S(2)}) copy-start(bf16[3,512]{1,0:T(4,128)(2,1)} %param.18) | copy-start | bytes 9220
  54.3 71.5 %all-to-all-start.1 = ((bf16[64,8,2048]{2,1,0:T(8,128)(2,1)}), bf16[64,8,2048]{2,1,0:T(8,128)(2,1)}, u32[]{:S(2)}, u32[]{:S(2)}) async-start(bf16[64,8,2048]{2,1,0:T(8,128)(2,1)} %bitcast_multiply_fusion), calls=%async_computation.2 | async-start | bytes 4194304 | tf_op jit(solution)/shard_map/all_to_all | solution.py:73
  76.0 127.5 %reduce-scatter.2.cloned.1.call-start = ((), (), s32[]{:S(2)}) async-start(), calls=%async_computation.4 | async-start | bytes 5242880 | tf_op jit(solution)/shard_map/reduce_scatter | solution.py:154
  76.1 4.7 %copy-start.12 = (bf16[512,512]{1,0:T(8,128)(2,1)S(1)}, bf16[512,512]{1,0:T(8,128)(2,1)}, u32[]{:S(2)}) copy-start(bf16[512,512]{1,0:T(8,128)(2,1)} %param.15) | copy-start | bytes 1572868
  76.2 4.4 %collective-permute-start = (bf16[2,2,512]{2,1,0:T(2,128)(2,1)S(1)}, bf16[2,2,512]{2,1,0:T(2,128)(2,1)S(1)}, u32[]{:S(2)}, u32[]{:S(2)}) collective-permute-start(bf16[2,2,512]{2,1,0:T(2,128)(2,1)S(1)} %pad_maximum_fusion.2), channel_id=1, source_target_pairs={{0,4},{4,8},{8,12},{12,16},{16,20},{20,24},{24,28},{28,32},{32,36}... | collective-permute-start | bytes 12296 | tf_op jit(solution)/shard_map/ppermute | solution.py:14
  80.8 2.8 %copy-start.10 = (bf16[2048,256]{1,0:T(8,128)(2,1)S(1)}, bf16[2048,256]{1,0:T(8,128)(2,1)}, u32[]{:S(2)}) copy-start(bf16[2048,256]{1,0:T(8,128)(2,1)} %param.25) | copy-start | bytes 3145732
  83.6 3.2 %copy-start.11 = (bf16[256,2048]{1,0:T(8,128)(2,1)S(1)}, bf16[256,2048]{1,0:T(8,128)(2,1)}, u32[]{:S(2)}) copy-start(bf16[256,2048]{1,0:T(8,128)(2,1)} %param.27) | copy-start | bytes 3145732
  86.9 5.8 %copy-start.3 = (bf16[512,2048]{1,0:T(8,128)(2,1)S(1)}, bf16[512,2048]{1,0:T(8,128)(2,1)}, u32[]{:S(2)}) copy-start(bf16[512,2048]{1,0:T(8,128)(2,1)} %convolution_convert_fusion.5) | copy-start | bytes 6291460
  150.1 6.4 %copy-start.4 = (bf16[1024,6144]{1,0:T(8,128)(2,1)S(1)}, bf16[1024,6144]{1,0:T(8,128)(2,1)}, u32[]{:S(2)}) copy-start(bf16[1024,6144]{1,0:T(8,128)(2,1)} %all-gather.2.cloned.1.call-done) | copy-start | bytes 37748740
  166.1 62.1 %all-to-all-start.2 = ((bf16[64,8,2048]{2,1,0:T(8,128)(2,1)}), bf16[64,8,2048]{2,1,0:T(8,128)(2,1)S(1)}, u32[]{:S(2)}, u32[]{:S(2)}) async-start(bf16[64,8,2048]{2,1,0:T(8,128)(2,1)} %fusion.2), calls=%async_computation.3 | async-start | bytes 4194304 | tf_op jit(solution)/shard_map/all_to_all | solution.py:164
  229.6 8.2 %copy-start.1 = (bf16[512,2048]{1,0:T(8,128)(2,1)S(1)}, bf16[512,2048]{1,0:T(8,128)(2,1)}, u32[]{:S(2)}) copy-start(bf16[512,2048]{1,0:T(8,128)(2,1)} %param.19) | copy-start | bytes 6291460
  231.9 4.9 %copy-start.5 = (bf16[256,2048]{1,0:T(8,128)(2,1)S(1)}, bf16[256,2048]{1,0:T(8,128)(2,1)}, u32[]{:S(2)}) copy-start(bf16[256,2048]{1,0:T(8,128)(2,1)} %reduce-scatter.2.cloned.1.call-done) | copy-start | bytes 3145732
Sparse Core Ops, SparseCore 0:
  14.3 135.8 all-gather.1
  152.7 50.7 reduce-scatter.1
where the time goes:
time: 246 us; the launch traced here: 245 us
  waiting for transfers between devices  120 us (49%)
  starting transfers between devices  42.9 us (17%)
  matrix products  26.1 us (11%)
  local copies, waits for them, and re-layouts  22.4 us (9%)
  other arithmetic  18.6 us (8%)
  between operations  14.3 us (6%)
    all_to_all x1, waiting for transfers between devices, send_own(): lax.all_to_all(outgoing, 'ep', split_axis=0, concat_axis=0, tiled=True)  29 us
    all_gather x1, waiting for transfers between devices, gather_turned(): result, at, outs = (lax.all_gather(both, axis, axis=0, tiled=True), 0, [])  24.3 us
    reduce_scatter x1, waiting for transfers between devices, per_device(): lax.psum_scatter(combined.reshape(dev_count * joint_block, model_width).a...  24.2 us
    all_to_all x1, waiting for transfers between devices, per_device(): lax.all_to_all(routed_back, 'ep', split_axis=0, concat_axis=0, tiled=True)  22.8 us
    all_to_all x1, starting transfers between devices, send_own(): lax.all_to_all(outgoing, 'ep', split_axis=0, concat_axis=0, tiled=True)  21.7 us
    all_to_all x1, waiting for transfers between devices, from_everyone(): lax.all_to_all(jnp.broadcast_to(array[None], (length, *array.shape)), axi...  19.5 us
    all_to_all x1, starting transfers between devices, per_device(): lax.all_to_all(routed_back, 'ep', split_axis=0, concat_axis=0, tiled=True)  12.4 us
    dot_general x2, matrix products, swiglu(): gate_term = jnp.dot(inputs, gate_w, preferred_element_type=jnp.float32)  8.57 us
  transfers between devices with their start and end apart: 6, of which 6 were waited for; matrix products, arithmetic and copies ran while one was open for 20% of the time, Pallas kernels for 0%

commit v1 on v0

v1 whole, which is shorter than its diff:
```python
import functools

import jax
import jax.numpy as jnp
from jax import lax
from jax.experimental import pallas as pl
from jax.experimental.pallas import tpu as pltpu
from jax.sharding import PartitionSpec as P

MESH = pl.DeviceIdType.MESH
epsilon = 1e-06
bf16 = jnp.bfloat16
f32 = jnp.float32
HALO = 16


def remote(src, dst, send_sem, recv_sem, ep, tp):
    return pltpu.make_async_remote_copy(
        src_ref=src,
        dst_ref=dst,
        send_sem=send_sem,
        recv_sem=recv_sem,
        device_id={"ep": ep, "tp": tp},
        device_id_type=MESH,
    )


def dot(a, b):
    return jnp.dot(a, b, preferred_element_type=f32)


def kernel(
    experts,
    capacity,
    tile,
    outer_hbm,
    inner_hbm,
    values_hbm,
    taps,
    outw_hbm,
    moe_hbm,
    gain,
    gate_hbm,
    up_hbm,
    down_hbm,
    sgate_hbm,
    sup_hbm,
    sdown_hbm,
    routes,
    weights,
    mixer_out,
    expert_out,
    moe,
    outer,
    inner,
    values,
    halo_inner,
    halo_values,
    product,
    gated,
    outw,
    group,
    outgoing,
    landed,
    results,
    returned,
    rows,
    wgate,
    wup,
    wdown,
    sgate,
    sup,
    sdown,
    act,
    sact,
    pick,
    spread_hi,
    spread_lo,
    mixer_part,
    shared_part,
    first_in,
    second_out,
    second_in,
    load_sem,
    halo_send,
    halo_recv,
    group_send,
    group_recv,
    out_send,
    out_recv,
    own_sem,
    far_send,
    near_send,
    twin_send,
    weight_recv,
    first_send,
    first_recv,
    second_send,
    second_recv,
    back_send,
    back_recv,
):
    ep, x = lax.axis_index("ep"), lax.axis_index("tp")
    core, chip = lax.rem(ep, 2), lax.div(ep, 2)
    near = x + 1 - 2 * lax.rem(x, 2)
    far = 3 - x
    side = lax.div(x, 2)
    owner = 1 - lax.rem(core + side, 2)
    own_index = ep * owner - (1 - owner)
    twin = ep + 1 - 2 * core
    plane = x + (far - x) * (1 - owner)
    mine = 2 * chip + side
    block, width = moe.shape
    length, channels = inner.shape
    units = sgate.shape[1]
    slots = experts * capacity

    loads = [
        (moe_hbm, moe),
        (inner_hbm, inner),
        (values_hbm, values),
        (outer_hbm, outer),
        (outw_hbm, outw),
        (sgate_hbm, sgate),
        (sup_hbm, sup),
        (sdown_hbm, sdown),
    ]
    loads = [pltpu.make_async_copy(s, d, load_sem.at[i]) for i, (s, d) in enumerate(loads)]
    loads[0].start()

    own_pieces = [gate_hbm.at[0], up_hbm.at[0], down_hbm.at[0]]
    held = [wgate, wup, wdown]

    def to_near(j):
        return remote(
            own_pieces[j], held[j].at[1], near_send.at[j], weight_recv.at[3 + j], ep, near
        )

    def to_far(j):
        return remote(own_pieces[j], held[j].at[2], far_send.at[j], weight_recv.at[6 + j], ep, far)

    def onward(j):
        return remote(
            held[j].at[2], held[j].at[3], near_send.at[3 + j], weight_recv.at[9 + j], ep, near
        )

    def to_twin(k, j):
        source = own_pieces[j] if k == 0 else held[j].at[k]
        return remote(
            source, held[j].at[k], twin_send.at[3 * k + j], weight_recv.at[3 * k + j], twin, x
        )

    def keep_own(j):
        return pltpu.make_async_copy(own_pieces[j], held[j].at[0], own_sem.at[j])

    @pl.when(owner == 1)
    def _():
        for j in range(3):
            to_near(j).start()

    @pl.when(owner == 0)
    def _():
        for j in range(3):
            to_far(j).start()

    after = lax.rem(ep + 1, experts)
    tail = pl.ds(length - HALO, HALO)
    halos = [
        remote(inner_hbm.at[tail], halo_inner, halo_send.at[0], halo_recv.at[0], after, x),
        remote(values_hbm.at[tail], halo_values, halo_send.at[1], halo_recv.at[1], after, x),
    ]
    for h in halos:
        h.start()

    at = pl.ds(pl.multiple_of(x * block, block), block)
    chosen = [routes[k : k + 1, at].astype(f32) for k in range(2)]
    expert_ids = lax.broadcasted_iota(jnp.int32, (experts, block), 0).astype(f32)
    hits = [(expert_ids == chosen[k]).astype(f32) for k in range(2)]
    earlier = (
        lax.broadcasted_iota(jnp.int32, (block, block), 0)
        < lax.broadcasted_iota(jnp.int32, (block, block), 1)
    ).astype(f32)
    rank = dot((hits[0] + hits[1]).astype(bf16), earlier.astype(bf16))
    place = [
        chosen[k] * capacity + jnp.sum(rank * hits[k], axis=0, keepdims=True) for k in range(2)
    ]
    slot_ids = lax.broadcasted_iota(jnp.int32, (slots, block), 0).astype(f32)
    pick[...] = ((slot_ids == place[0]).astype(f32) + (slot_ids == place[1]).astype(f32)).astype(
        bf16
    )

    loads[0].wait()
    step = min(16, block)

    @pl.loop(0, block // step)
    def _(i):
        r = pl.ds(pl.multiple_of(i * step, step), step)
        v = moe[r, :].astype(f32)
        square = jnp.mean(v * v, axis=-1, keepdims=True)
        group[x, r, :] = (v * lax.rsqrt(square + epsilon) * gain[...].astype(f32)).astype(bf16)

    @pl.loop(0, width // tile)
    def _(i):
        cols = pl.ds(pl.multiple_of(i * tile, tile), tile)
        taken = dot(pick[...], group[x, :, cols])
        outgoing[:, :, cols] = taken.reshape(experts, capacity, tile).astype(bf16)

    def send_out(e):
        cross = lax.rem(lax.rem(e, 2) + side, 2)
        return remote(
            outgoing.at[e],
            landed.at[ep],
            out_send.at[0],
            out_recv.at[0],
            2 * lax.div(e, 2) + side,
            x + (far - x) * cross,
        )

    @pl.loop(0, experts)
    def _(i):
        e = lax.rem(ep + 1 + i, experts)

        @pl.when(e != own_index)
        def _():
            send_out(e).start()

    group_copies = [
        remote(group.at[x], group.at[x], group_send.at[0], group_recv.at[0], ep, near),
        remote(group.at[x], group.at[x], group_send.at[1], group_recv.at[1], ep, far),
        remote(group.at[near], group.at[near], group_send.at[2], group_recv.at[2], ep, far),
    ]
    group_copies[0].start()
    group_copies[1].start()

    @pl.when(owner == 1)
    def _():
        for j in range(3):
            to_twin(0, j).start()
            keep_own(j).start()

    for c in loads[1:]:
        c.start()

    def relay(j):
        @pl.when(owner == 1)
        def _():
            to_far(j).wait_recv()
            onward(j).start()
            to_twin(2, j).start()
            to_near(j).wait_recv()
            to_twin(1, j).start()

    @pl.when(owner == 1)
    def _():
        landed[ep] = outgoing[ep]

    share = [weights[k : k + 1, at] for k in range(2)]
    spread = jnp.where(slot_ids == place[0], share[0], 0.0) + jnp.where(
        slot_ids == place[1], share[1], 0.0
    )
    spread = spread.T
    high = spread.astype(bf16)
    spread_hi[...] = high
    spread_lo[...] = (spread - high.astype(f32)).astype(bf16)

    for c in loads[1:4]:
        c.wait()
    for h in halos:
        h.wait_recv()
    first = (ep > 0).astype(f32)
    product[0:HALO, :] = halo_inner[...].astype(f32) * halo_values[...].astype(f32) * first
    piece = min(64, length)

    @pl.loop(0, length // piece)
    def _(i):
        r = pl.ds(pl.multiple_of(i * piece, piece), piece)
        product[pl.ds(pl.multiple_of(HALO + i * piece, HALO), piece), :] = inner[r, :].astype(
            f32
        ) * values[r, :].astype(f32)

    tap = taps[...].astype(f32)
    for i in range(length // piece):
        lo = i * piece
        conv = tap[0:1] * product[HALO - 2 + lo : HALO - 2 + lo + piece, :]
        conv = conv + tap[1:2] * product[HALO - 1 + lo : HALO - 1 + lo + piece, :]
        conv = conv + tap[2:3] * product[HALO + lo : HALO + lo + piece, :]
        gated[lo : lo + piece, :] = (outer[lo : lo + piece, :].astype(f32) * conv).astype(bf16)
    loads[4].wait()

    @pl.loop(0, width // tile)
    def _(i):
        cols = pl.ds(pl.multiple_of(i * tile, tile), tile)
        part = dot(gated[...], outw[:, cols]).astype(bf16)
        mixer_part[:, :, cols] = part.reshape(4, block, tile)

    relay(0)

    group_copies[0].wait_recv()
    group_copies[2].start()
    group_copies[1].wait_recv()
    relay(1)
    group_copies[2].wait_recv()
    for c in loads[5:8]:
        c.wait()

    @pl.loop(0, 4)
    def _(b):
        g = dot(group[b], sgate[...])
        u = dot(group[b], sup[...])
        r = pl.ds(pl.multiple_of(b * block, block), block)
        sact[r, :] = (g / (1.0 + jnp.exp(-g)) * u).astype(bf16)

    @pl.loop(0, width // tile)
    def _(i):
        cols = pl.ds(pl.multiple_of(i * tile, tile), tile)
        part = dot(sact[...], sdown[:, cols]).astype(bf16)
        shared_part[:, :, cols] = part.reshape(4, block, tile)

    relay(2)

    @pl.when(owner == 1)
    def _():
        some = landed.at[pl.ds(0, experts - 1)]
        remote(some, some, out_send.at[0], out_recv.at[0], twin, x).wait_recv()

    @pl.when(owner == 0)
    def _():
        remote(landed, landed, out_send.at[0], out_recv.at[0], twin, x).wait_recv()

    half = slots // 2
    half_experts = experts // 2

    @pl.loop(0, width // tile)
    def _(i):
        cols = pl.ds(pl.multiple_of(i * tile, tile), tile)
        rows[:, cols] = landed[:, :, cols].reshape(slots, tile)

    def gate_up(k):
        cols = pl.ds(pl.multiple_of(k * units, units), units)

        @pl.loop(0, 2)
        def _(m):
            r = pl.ds(pl.multiple_of(m * half, half), half)
            g = dot(rows[r, :], wgate[k])
            u = dot(rows[r, :], wup[k])
            act[r, cols] = (g / (1.0 + jnp.exp(-g)) * u).astype(bf16)

    for k in range(3):

        @pl.when(owner == 0)
        def _():
            for j in range(2):
                to_twin(k, j).wait_recv()

        if k == 0:

            @pl.when(owner == 1)
            def _():
                for j in range(2):
                    keep_own(j).wait()

        gate_up(k)

    for j in range(2):

        @pl.when(owner == 1)
        def _():
            onward(j).wait_recv()
            to_twin(3, j).start()

        @pl.when(owner == 0)
        def _():
            to_twin(3, j).wait_recv()

    gate_up(3)

    @pl.when(owner == 1)
    def _():
        keep_own(2).wait()
        onward(2).wait_recv()
        to_twin(3, 2).start()

    @pl.when(owner == 0)
    def _():
        for k in range(4):
            to_twin(k, 2).wait_recv()

    def send_back(s):
        return remote(
            results.at[s], returned.at[mine], back_send.at[0], back_recv.at[0], s, plane
        )

    @pl.loop(0, 2)
    def _(m):
        r = pl.ds(pl.multiple_of(m * half, half), half)

        @pl.loop(0, width // tile)
        def _(i):
            cols = pl.ds(pl.multiple_of(i * tile, tile), tile)
            total = dot(act[r, 0:units], wdown[0, :, cols])
            for k in range(1, 4):
                total = total + dot(act[r, k * units : (k + 1) * units], wdown[k, :, cols])
            results[pl.ds(m * half_experts, half_experts), :, cols] = total.reshape(
                half_experts, capacity, tile
            ).astype(bf16)

        @pl.loop(0, half_experts)
        def _(i):
            s = m * half_experts + lax.rem(ep + 1 + i, half_experts)

            @pl.when(s != own_index)
            def _():
                send_back(s).start()

    parts = [mixer_part, shared_part]

    def first_copy(kind, b):
        src = near if b == 0 else 3 - near
        return remote(
            parts[kind].at[src],
            first_in.at[kind, b],
            first_send.at[2 * kind + b],
            first_recv.at[2 * kind + b],
            ep,
            near,
        )

    def second_copy(kind):
        return remote(
            second_out.at[kind],
            second_in.at[kind],
            second_send.at[kind],
            second_recv.at[kind],
            ep,
            far,
        )

    for kind in range(2):
        for b in (1, 0):
            first_copy(kind, b).start()

    @pl.when(owner == 1)
    def _():
        returned[ep] = results[ep]

    pieces = 4 if block % 64 == 0 else 1
    some_rows = block // pieces

    for kind in range(2):
        first_copy(kind, 1).wait_recv()

        @pl.loop(0, pieces)
        def _(i):
            r = pl.ds(pl.multiple_of(i * some_rows, some_rows), some_rows)
            second_out[kind, r, :] = (
                parts[kind][far, r, :].astype(f32) + first_in[kind, 1, r, :].astype(f32)
            ).astype(bf16)

        second_copy(kind).start()

    first_copy(0, 0).wait_recv()
    second_copy(0).wait_recv()

    @pl.loop(0, pieces)
    def _(i):
        r = pl.ds(pl.multiple_of(i * some_rows, some_rows), some_rows)
        mixer_out[r, :] = (
            mixer_part[x, r, :].astype(f32)
            + first_in[0, 0, r, :].astype(f32)
            + second_in[0, r, :].astype(f32)
        ).astype(bf16)

    first_copy(1, 0).wait_recv()
    second_copy(1).wait_recv()

    @pl.when(owner == 1)
    def _():
        some = returned.at[pl.ds(0, experts - 1)]
        remote(some, some, back_send.at[0], back_recv.at[0], twin, x).wait_recv()

    @pl.when(owner == 0)
    def _():
        remote(returned, returned, back_send.at[0], back_recv.at[0], twin, x).wait_recv()

    @pl.loop(0, width // tile)
    def _(i):
        cols = pl.ds(pl.multiple_of(i * tile, tile), tile)
        back = returned[:, :, cols].reshape(slots, tile)
        total = (
            shared_part[x, :, cols].astype(f32)
            + first_in[1, 0, :, cols].astype(f32)
            + second_in[1, :, cols].astype(f32)
        )
        total = total + dot(spread_hi[...], back) + dot(spread_lo[...], back)
        expert_out[:, cols] = total.astype(bf16)

    for h in halos:
        h.wait_send()
    for c in group_copies:
        c.wait_send()
    for kind in range(2):
        for b in range(2):
            first_copy(kind, b).wait_send()
        second_copy(kind).wait_send()

    @pl.when(owner == 1)
    def _():
        for j in range(3):
            to_near(j).wait_send()
            onward(j).wait_send()
            for k in range(4):
                to_twin(k, j).wait_send()
        some = outgoing.at[pl.ds(0, experts - 1)]
        remote(some, some, out_send.at[0], out_recv.at[0], twin, x).wait_send()
        some = results.at[pl.ds(0, experts - 1)]
        remote(some, some, back_send.at[0], back_recv.at[0], twin, x).wait_send()

    @pl.when(owner == 0)
    def _():
        for j in range(3):
            to_far(j).wait_send()
        remote(outgoing, outgoing, out_send.at[0], out_recv.at[0], twin, x).wait_send()
        remote(results, results, back_send.at[0], back_recv.at[0], twin, x).wait_send()


def per_device(
    outer_gate,
    inner_gate,
    conv_values,
    conv_taps,
    out_weight,
    moe_input,
    norm_gain,
    gate_proj,
    up_proj,
    down_proj,
    shared_gate,
    shared_up,
    shared_down,
    routes,
    route_weight,
):
    experts = lax.axis_size("ep")
    length, channels = inner_gate.shape
    block, width = moe_input.shape
    units = gate_proj.shape[2]
    capacity = 2 * block * routes.shape[1] // experts
    slots = experts * capacity
    tile = min(256, width)
    vmem = pl.BlockSpec(memory_space=pltpu.VMEM)
    hbm = pl.BlockSpec(memory_space=pl.ANY)
    dma = pltpu.SemaphoreType.DMA

    def space(*shape):
        return pltpu.VMEM(shape, bf16)

    out = jax.ShapeDtypeStruct((block, width), bf16)
    return pl.pallas_call(
        functools.partial(kernel, experts, capacity, tile),
        name="whole",
        out_shape=(out, out),
        in_specs=[hbm, hbm, hbm, vmem, hbm, hbm, vmem] + [hbm] * 6 + [vmem, vmem],
        out_specs=(vmem, vmem),
        scratch_shapes=[
            space(block, width),
            space(length, channels),
            space(length, channels),
            space(length, channels),
            space(HALO, channels),
            space(HALO, channels),
            pltpu.VMEM((HALO + length, channels), f32),
            space(length, channels),
            space(channels, width),
            space(4, block, width),
            space(experts, capacity, width),
            space(experts, capacity, width),
            space(experts, capacity, width),
            space(experts, capacity, width),
            space(slots, width),
            space(4, width, units),
            space(4, width, units),
            space(4, units, width),
            space(width, units),
            space(width, units),
            space(units, width),
            space(slots, 4 * units),
            space(4 * block, units),
            space(slots, block),
            space(block, slots),
            space(block, slots),
            space(4, block, width),
            space(4, block, width),
            space(2, 2, block, width),
            space(2, block, width),
            space(2, block, width),
            dma((8,)),
            dma((2,)),
            dma((2,)),
            dma((3,)),
            dma((3,)),
            dma((1,)),
            dma((1,)),
            dma((3,)),
            dma((3,)),
            dma((6,)),
            dma((12,)),
            dma((12,)),
            dma((4,)),
            dma((4,)),
            dma((2,)),
            dma((2,)),
            dma((1,)),
            dma((1,)),
        ],
        compiler_params=pltpu.CompilerParams(
            has_side_effects=True, vmem_limit_bytes=60 * 1024 * 1024
        ),
    )(
        outer_gate,
        inner_gate,
        conv_values,
        conv_taps,
        out_weight,
        moe_input,
        norm_gain.reshape(1, width),
        gate_proj,
        up_proj,
        down_proj,
        shared_gate,
        shared_up,
        shared_down,
        routes.T,
        route_weight.T,
    )


def solution(mesh):
    return jax.shard_map(
        per_device,
        mesh=mesh,
        in_specs=(
            P("ep", "tp"),
            P("ep", "tp"),
            P("ep", "tp"),
            P(None, "tp"),
            P("tp", None),
            P(("ep", "tp"), None),
            P(),
            P("ep", None, "tp"),
            P("ep", None, "tp"),
            P("ep", "tp", None),
            P(None, "tp"),
            P(None, "tp"),
            P("tp", None),
            P("ep", None),
            P("ep", None),
        ),
        out_specs=(P(("ep", "tp"), None), P(("ep", "tp"), None)),
        check_vma=False,
    )
```

time: 246 us -> 189 us (0.77)
  the two profiles are of different devices: /device:TPU:1 before, /device:TPU:229 now
where the time goes in v1:
time: 189 us
  Pallas kernels  183 us (97%)
  local copies, waits for them, and re-layouts  5.05 us (3%)
    pallas_call x1, Pallas kernels, per_device(): pl.pallas_call(functools.partial(kernel, experts, capacity, tile), name='...  183 us

profile of v1, /device:TPU:229, one launch (start us, length us, event | category | flops | bytes accessed | tf_op | source)
XLA Modules:
  0.0 188.5 jit_solution(4822589143434206335)
XLA Ops:
  0.6 1.3 reshape.7.gain
  1.9 182.9 %whole.1 = (bf16[128,2048]{1,0:T(8,128)(2,1)}, bf16[128,2048]{1,0:T(8,128)(2,1)}) custom-call(bf16[512,512]{1,0:T(8,128)(2,1)} %outer_hbm.1, bf16[512,512]{1,0:T(8,128)(2,1)} %inner_hbm.1, bf16[512,512]{1,0:T(8,128)(2,1)} %values_hbm.1, bf16[3,512]{1,0:T(4,128)(2,1)} %taps.1, bf16[512,2048]{1,0:T(8,128)(2,1)} %outw_hbm.1, bf16[128,2048]{1,0:T(8,128)(2,1)} %moe_hbm.1, ...), custom_call_target="tpu_custom_call" | custom-call | tf_op jit(solution)/shard_map/whole/pallas_call | solution.py:558
  184.8 1.9 copy.19
  186.7 1.9 copy.20

commit v2 on v1

--- a/solution.py
+++ b/solution.py
@@ -153,15 +153,36 @@
     def keep_own(j):
         return pltpu.make_async_copy(own_pieces[j], held[j].at[0], own_sem.at[j])
 
+    barrier = pltpu.get_barrier_semaphore()
+
+    def greet(device, tp):
+        pl.semaphore_signal(
+            barrier, inc=1, device_id={"ep": device, "tp": tp}, device_id_type=MESH
+        )
+
+    greet(ep, near)
+    greet(ep, far)
+    greet(lax.rem(ep + experts - 1, experts), x)
+
+    @pl.when(owner == 0)
+    def _():
+        greet(twin, x)
+
+    @pl.loop(0, experts)
+    def _(i):
+        s = lax.rem(ep + 1 + i, experts)
+
+        @pl.when(s != own_index)
+        def _():
+            greet(s, plane)
+
     @pl.when(owner == 1)
     def _():
         for j in range(3):
-            to_near(j).start()
-
-    @pl.when(owner == 0)
-    def _():
-        for j in range(3):
-            to_far(j).start()
+            keep_own(j).start()
+
+    for c in loads[1:]:
+        c.start()
 
     after = lax.rem(ep + 1, experts)
     tail = pl.ds(length - HALO, HALO)
@@ -169,8 +190,6 @@
         remote(inner_hbm.at[tail], halo_inner, halo_send.at[0], halo_recv.at[0], after, x),
         remote(values_hbm.at[tail], halo_values, halo_send.at[1], halo_recv.at[1], after, x),
     ]
-    for h in halos:
-        h.start()
 
     at = pl.ds(pl.multiple_of(x * block, block), block)
     chosen = [routes[k : k + 1, at].astype(f32) for k in range(2)]
@@ -190,6 +209,7 @@
     )
 
     loads[0].wait()
+    scale = gain[...].reshape(1, width).astype(f32)
     step = min(16, block)
 
     @pl.loop(0, block // step)
@@ -197,7 +217,7 @@
         r = pl.ds(pl.multiple_of(i * step, step), step)
         v = moe[r, :].astype(f32)
         square = jnp.mean(v * v, axis=-1, keepdims=True)
-        group[x, r, :] = (v * lax.rsqrt(square + epsilon) * gain[...].astype(f32)).astype(bf16)
+        group[x, r, :] = (v * lax.rsqrt(square + epsilon) * scale).astype(bf16)
 
     @pl.loop(0, width // tile)
     def _(i):
@@ -216,6 +236,10 @@
             x + (far - x) * cross,
         )
 
+    pl.semaphore_wait(barrier, experts + 3)
+    for h in halos:
+        h.start()
+
     @pl.loop(0, experts)
     def _(i):
         e = lax.rem(ep + 1 + i, experts)
@@ -223,23 +247,24 @@
         @pl.when(e != own_index)
         def _():
             send_out(e).start()
+
+    @pl.when(owner == 1)
+    def _():
+        for j in range(3):
+            to_near(j).start()
+        for j in range(3):
+            to_twin(0, j).start()
+
+    @pl.when(owner == 0)
+    def _():
+        for j in range(3):
+            to_far(j).start()
 
     group_copies = [
         remote(group.at[x], group.at[x], group_send.at[0], group_recv.at[0], ep, near),
         remote(group.at[x], group.at[x], group_send.at[1], group_recv.at[1], ep, far),
         remote(group.at[near], group.at[near], group_send.at[2], group_recv.at[2], ep, far),
     ]
-    group_copies[0].start()
-    group_copies[1].start()
-
-    @pl.when(owner == 1)
-    def _():
-        for j in range(3):
-            to_twin(0, j).start()
-            keep_own(j).start()
-
-    for c in loads[1:]:
-        c.start()
 
     def relay(j):
         @pl.when(owner == 1)
@@ -295,27 +320,7 @@
 
     relay(0)
 
-    group_copies[0].wait_recv()
-    group_copies[2].start()
-    group_copies[1].wait_recv()
     relay(1)
-    group_copies[2].wait_recv()
-    for c in loads[5:8]:
-        c.wait()
-
-    @pl.loop(0, 4)
-    def _(b):
-        g = dot(group[b], sgate[...])
-        u = dot(group[b], sup[...])
-        r = pl.ds(pl.multiple_of(b * block, block), block)
-        sact[r, :] = (g / (1.0 + jnp.exp(-g)) * u).astype(bf16)
-
-    @pl.loop(0, width // tile)
-    def _(i):
-        cols = pl.ds(pl.multiple_of(i * tile, tile), tile)
-        part = dot(sact[...], sdown[:, cols]).astype(bf16)
-        shared_part[:, :, cols] = part.reshape(4, block, tile)
-
     relay(2)
 
     @pl.when(owner == 1)
@@ -373,6 +378,34 @@
             to_twin(3, j).wait_recv()
 
     gate_up(3)
+
+    parts = [mixer_part, shared_part]
+
+    def first_copy(kind, b):
+        src = near if b == 0 else 3 - near
+        return remote(
+            parts[kind].at[src],
+            first_in.at[kind, b],
+            first_send.at[2 * kind + b],
+            first_recv.at[2 * kind + b],
+            ep,
+            near,
+        )
+
+    def second_copy(kind):
+        return remote(
+            second_out.at[kind],
+            second_in.at[kind],
+            second_send.at[kind],
+            second_recv.at[kind],
+            ep,
+            far,
+        )
+
+    group_copies[0].start()
+    group_copies[1].start()
+    for b in (1, 0):
+        first_copy(0, b).start()
 
     @pl.when(owner == 1)
     def _():
@@ -412,32 +445,28 @@
             def _():
                 send_back(s).start()
 
-    parts = [mixer_part, shared_part]
-
-    def first_copy(kind, b):
-        src = near if b == 0 else 3 - near
-        return remote(
-            parts[kind].at[src],
-            first_in.at[kind, b],
-            first_send.at[2 * kind + b],
-            first_recv.at[2 * kind + b],
-            ep,
-            near,
-        )
-
-    def second_copy(kind):
-        return remote(
-            second_out.at[kind],
-            second_in.at[kind],
-            second_send.at[kind],
-            second_recv.at[kind],
-            ep,
-            far,
-        )
-
-    for kind in range(2):
-        for b in (1, 0):
-            first_copy(kind, b).start()
+    group_copies[0].wait_recv()
+    group_copies[2].start()
+    group_copies[1].wait_recv()
+    group_copies[2].wait_recv()
+    for c in loads[5:8]:
+        c.wait()
+
+    @pl.loop(0, 4)
+    def _(b):
+        g = dot(group[b], sgate[...])
+        u = dot(group[b], sup[...])
+        r = pl.ds(pl.multiple_of(b * block, block), block)
+        sact[r, :] = (g / (1.0 + jnp.exp(-g)) * u).astype(bf16)
+
+    @pl.loop(0, width // tile)
+    def _(i):
+        cols = pl.ds(pl.multiple_of(i * tile, tile), tile)
+        part = dot(sact[...], sdown[:, cols]).astype(bf16)
+        shared_part[:, :, cols] = part.reshape(4, block, tile)
+
+    for b in (1, 0):
+        first_copy(1, b).start()
 
     @pl.when(owner == 1)
     def _():
@@ -613,7 +642,7 @@
             dma((1,)),
         ],
         compiler_params=pltpu.CompilerParams(
-            has_side_effects=True, vmem_limit_bytes=60 * 1024 * 1024
+            collective_id=0, has_side_effects=True, vmem_limit_bytes=60 * 1024 * 1024
         ),
     )(
         outer_gate,
@@ -622,7 +651,7 @@
         conv_taps,
         out_weight,
         moe_input,
-        norm_gain.reshape(1, width),
+        norm_gain,
         gate_proj,
         up_proj,
         down_proj,

time: 189 us -> 168 us (0.89)
  the two profiles are of different devices: /device:TPU:229 before, /device:TPU:1 now
where the time goes in v2:
time: 168 us; the launch traced here: 166 us
  Pallas kernels  162 us (96%)
  local copies, waits for them, and re-layouts  3.76 us (2%)
    pallas_call x1, Pallas kernels, per_device(): pl.pallas_call(functools.partial(kernel, experts, capacity, tile), name='...  162 us
    unnamed x2, local copies, waits for them, and re-layouts  3.76 us

profile of v2, /device:TPU:1, one launch (start us, length us, event | category | flops | bytes accessed | tf_op | source)
XLA Modules:
  0.0 166.2 jit_solution(16935750312535748364)
XLA Ops:
  0.6 161.8 %whole.1 = (bf16[128,2048]{1,0:T(8,128)(2,1)}, bf16[128,2048]{1,0:T(8,128)(2,1)}) custom-call(bf16[512,512]{1,0:T(8,128)(2,1)} %outer_hbm.1, bf16[512,512]{1,0:T(8,128)(2,1)} %inner_hbm.1, bf16[512,512]{1,0:T(8,128)(2,1)} %values_hbm.1, bf16[3,512]{1,0:T(4,128)(2,1)} %taps.1, bf16[512,2048]{1,0:T(8,128)(2,1)} %outw_hbm.1, bf16[128,2048]{1,0:T(8,128)(2,1)} %moe_hbm.1, ...), custom_call_target="tpu_custom_call" | custom-call | tf_op jit(solution)/shard_map/whole/pallas_call | solution.py:587
  162.5 1.9 %copy.19 = bf16[128,2048]{1,0:T(8,128)(2,1)} copy(bf16[128,2048]{1,0:T(8,128)(2,1)} %get-tuple-element.4) | data formatting | bytes 1048576
  164.4 1.9 %copy.20 = bf16[128,2048]{1,0:T(8,128)(2,1)} copy(bf16[128,2048]{1,0:T(8,128)(2,1)} %get-tuple-element.5) | data formatting | bytes 1048576

commit v3 on v2

--- a/solution.py
+++ b/solution.py
@@ -32,6 +32,7 @@
 def kernel(
     experts,
     capacity,
+    rings,
     tile,
     outer_hbm,
     inner_hbm,
@@ -76,8 +77,11 @@
     pick,
     spread_hi,
     spread_lo,
+    total_down,
     mixer_part,
-    shared_part,
+    shared_own,
+    shared_near,
+    shared_in,
     first_in,
     second_out,
     second_in,
@@ -97,6 +101,12 @@
     first_recv,
     second_send,
     second_recv,
+    shared_send,
+    shared_recv,
+    eighth_send,
+    ring_send,
+    pass_send,
+    eighth_recv,
     back_send,
     back_recv,
 ):
@@ -112,7 +122,11 @@
     mine = 2 * chip + side
     block, width = moe.shape
     length, channels = inner.shape
-    units = sgate.shape[1]
+    units = sgate.shape[2]
+    own_rows, near_rows = pl.ds(0, block), pl.ds(block, block)
+    y = lax.rem(chip, rings)
+    eighths = 2 * rings
+    eighth = 2 * y + core
     slots = experts * capacity
 
     loads = [
@@ -121,9 +135,9 @@
         (values_hbm, values),
         (outer_hbm, outer),
         (outw_hbm, outw),
-        (sgate_hbm, sgate),
-        (sup_hbm, sup),
-        (sdown_hbm, sdown),
+        (sgate_hbm, sgate.at[0]),
+        (sup_hbm, sup.at[0]),
+        (sdown_hbm, sdown.at[pl.ds(0, units)]),
     ]
     loads = [pltpu.make_async_copy(s, d, load_sem.at[i]) for i, (s, d) in enumerate(loads)]
     loads[0].start()
@@ -164,9 +178,9 @@
     greet(ep, far)
     greet(lax.rem(ep + experts - 1, experts), x)
 
-    @pl.when(owner == 0)
-    def _():
-        greet(twin, x)
+    greet(twin, x)
+    for d in range(1, rings):
+        greet(2 * (chip - y + lax.rem(y + d, rings)) + core, x)
 
     @pl.loop(0, experts)
     def _(i):
@@ -217,12 +231,12 @@
         r = pl.ds(pl.multiple_of(i * step, step), step)
         v = moe[r, :].astype(f32)
         square = jnp.mean(v * v, axis=-1, keepdims=True)
-        group[x, r, :] = (v * lax.rsqrt(square + epsilon) * scale).astype(bf16)
+        group[r, :] = (v * lax.rsqrt(square + epsilon) * scale).astype(bf16)
 
     @pl.loop(0, width // tile)
     def _(i):
         cols = pl.ds(pl.multiple_of(i * tile, tile), tile)
-        taken = dot(pick[...], group[x, :, cols])
+        taken = dot(pick[...], group[own_rows, cols])
         outgoing[:, :, cols] = taken.reshape(experts, capacity, tile).astype(bf16)
 
     def send_out(e):
@@ -236,7 +250,7 @@
             x + (far - x) * cross,
         )
 
-    pl.semaphore_wait(barrier, experts + 3)
+    pl.semaphore_wait(barrier, experts + 3 + rings - owner)
     for h in halos:
         h.start()
 
@@ -248,6 +262,57 @@
         def _():
             send_out(e).start()
 
+    shared_hbm = [sgate_hbm, sup_hbm, sdown_hbm]
+
+    def held_eighth(j, i):
+        n = shared_hbm[j].shape[0] // eighths
+        if j < 2:
+            return [sgate, sup][j].at[1, pl.ds(pl.multiple_of(i * n, n), n)]
+        return sdown.at[pl.ds(pl.multiple_of(units + i * n, n), n)]
+
+    def to_far_eighth(j):
+        n = shared_hbm[j].shape[0] // eighths
+        return remote(
+            shared_hbm[j].at[pl.ds(pl.multiple_of(eighth * n, n), n)],
+            held_eighth(j, eighth),
+            eighth_send.at[j],
+            eighth_recv.at[3 * eighth + j],
+            ep,
+            far,
+        )
+
+    def round_ring(j, d):
+        return remote(
+            held_eighth(j, eighth),
+            held_eighth(j, eighth),
+            ring_send.at[3 * d + j],
+            eighth_recv.at[3 * eighth + j],
+            2 * (chip - y + lax.rem(y + d, rings)) + core,
+            x,
+        )
+
+    def from_ring(j, d):
+        i = 2 * lax.rem(y + d, rings) + core
+        return remote(
+            held_eighth(j, i),
+            held_eighth(j, i),
+            pass_send.at[3 * d + j],
+            eighth_recv.at[3 * i + j],
+            twin,
+            x,
+        )
+
+    def from_twin(j, d):
+        i = 2 * lax.rem(y + d, rings) + 1 - core
+        return remote(
+            held_eighth(j, i),
+            held_eighth(j, i),
+            pass_send.at[3 * d + j],
+            eighth_recv.at[3 * i + j],
+            twin,
+            x,
+        )
+
     @pl.when(owner == 1)
     def _():
         for j in range(3):
@@ -259,12 +324,8 @@
     def _():
         for j in range(3):
             to_far(j).start()
-
-    group_copies = [
-        remote(group.at[x], group.at[x], group_send.at[0], group_recv.at[0], ep, near),
-        remote(group.at[x], group.at[x], group_send.at[1], group_recv.at[1], ep, far),
-        remote(group.at[near], group.at[near], group_send.at[2], group_recv.at[2], ep, far),
-    ]
+        for j in range(3):
+            to_far_eighth(j).start()
 
     def relay(j):
         @pl.when(owner == 1)
@@ -323,6 +384,20 @@
     relay(1)
     relay(2)
 
+    def passed(j):
+        @pl.when(owner == 1)
+        def _():
+            onward(j).wait_recv()
+            to_twin(3, j).start()
+
+    @pl.when(owner == 1)
+    def _():
+        for j in range(3):
+            to_far_eighth(j).start()
+
+    passed(0)
+
+
     @pl.when(owner == 1)
     def _():
         some = landed.at[pl.ds(0, experts - 1)]
@@ -333,7 +408,6 @@
         remote(landed, landed, out_send.at[0], out_recv.at[0], twin, x).wait_recv()
 
     half = slots // 2
-    half_experts = experts // 2
 
     @pl.loop(0, width // tile)
     def _(i):
@@ -365,13 +439,29 @@
                     keep_own(j).wait()
 
         gate_up(k)
+        if k == 1:
+            passed(1)
+
+    @pl.when(owner == 0)
+    def _():
+        for k in range(3):
+            to_twin(k, 2).wait_recv()
+
+    @pl.when(owner == 1)
+    def _():
+        keep_own(2).wait()
+
+    @pl.loop(0, width // tile)
+    def _(i):
+        cols = pl.ds(pl.multiple_of(i * tile, tile), tile)
+        for m in range(2):
+            r = pl.ds(m * half, half)
+            total = dot(act[r, 0:units], wdown[0, :, cols])
+            for k in range(1, 3):
+                total = total + dot(act[r, k * units : (k + 1) * units], wdown[k, :, cols])
+            total_down[r, cols] = total
 
     for j in range(2):
-
-        @pl.when(owner == 1)
-        def _():
-            onward(j).wait_recv()
-            to_twin(3, j).start()
 
         @pl.when(owner == 0)
         def _():
@@ -379,128 +469,130 @@
 
     gate_up(3)
 
-    parts = [mixer_part, shared_part]
-
-    def first_copy(kind, b):
+    group_copy = remote(
+        group.at[own_rows], group.at[near_rows], group_send.at[0], group_recv.at[0], ep, near
+    )
+
+    def first_copy(b):
         src = near if b == 0 else 3 - near
         return remote(
-            parts[kind].at[src],
-            first_in.at[kind, b],
-            first_send.at[2 * kind + b],
-            first_recv.at[2 * kind + b],
-            ep,
-            near,
-        )
-
-    def second_copy(kind):
-        return remote(
-            second_out.at[kind],
-            second_in.at[kind],
-            second_send.at[kind],
-            second_recv.at[kind],
-            ep,
-            far,
-        )
-
-    group_copies[0].start()
-    group_copies[1].start()
+            mixer_part.at[src], first_in.at[b], first_send.at[b], first_recv.at[b], ep, near
+        )
+
+    second_copy = remote(
+        second_out, second_in, second_send.at[0], second_recv.at[0], ep, far
+    )
+    shared_copy = remote(
+        shared_near, shared_in, shared_send.at[0], shared_recv.at[0], ep, near
+    )
+
+    group_copy.start()
     for b in (1, 0):
-        first_copy(0, b).start()
-
-    @pl.when(owner == 1)
-    def _():
-        keep_own(2).wait()
-        onward(2).wait_recv()
-        to_twin(3, 2).start()
+        first_copy(b).start()
+
+    for j in range(3):
+        to_far_eighth(j).wait_recv()
+        for d in range(1, rings):
+            round_ring(j, d).start()
+        from_ring(j, 0).start()
+
+    passed(2)
 
     @pl.when(owner == 0)
     def _():
-        for k in range(4):
-            to_twin(k, 2).wait_recv()
+        to_twin(3, 2).wait_recv()
 
     def send_back(s):
         return remote(
             results.at[s], returned.at[mine], back_send.at[0], back_recv.at[0], s, plane
         )
 
-    @pl.loop(0, 2)
+    chunks = 4 if slots % 64 == 0 and experts % 4 == 0 else 1
+    chunk, chunk_experts = slots // chunks, experts // chunks
+
+    @pl.loop(0, chunks)
     def _(m):
-        r = pl.ds(pl.multiple_of(m * half, half), half)
+        r = pl.ds(pl.multiple_of(m * chunk, chunk), chunk)
 
         @pl.loop(0, width // tile)
         def _(i):
             cols = pl.ds(pl.multiple_of(i * tile, tile), tile)
-            total = dot(act[r, 0:units], wdown[0, :, cols])
-            for k in range(1, 4):
-                total = total + dot(act[r, k * units : (k + 1) * units], wdown[k, :, cols])
-            results[pl.ds(m * half_experts, half_experts), :, cols] = total.reshape(
-                half_experts, capacity, tile
+            total = total_down[r, cols] + dot(act[r, 3 * units : 4 * units], wdown[3, :, cols])
+            results[pl.ds(m * chunk_experts, chunk_experts), :, cols] = total.reshape(
+                chunk_experts, capacity, tile
             ).astype(bf16)
 
-        @pl.loop(0, half_experts)
+        @pl.loop(0, chunk_experts)
         def _(i):
-            s = m * half_experts + lax.rem(ep + 1 + i, half_experts)
+            s = m * chunk_experts + lax.rem(ep + 1 + i, chunk_experts)
 
             @pl.when(s != own_index)
             def _():
                 send_back(s).start()
 
-    group_copies[0].wait_recv()
-    group_copies[2].start()
-    group_copies[1].wait_recv()
-    group_copies[2].wait_recv()
+    @pl.when(owner == 1)
+    def _():
+        returned[ep] = results[ep]
+
+    for d in range(1, rings):
+        for j in range(3):
+            from_ring(j, d).wait_recv()
+            from_ring(j, d).start()
+
+    group_copy.wait_recv()
     for c in loads[5:8]:
         c.wait()
 
-    @pl.loop(0, 4)
-    def _(b):
-        g = dot(group[b], sgate[...])
-        u = dot(group[b], sup[...])
-        r = pl.ds(pl.multiple_of(b * block, block), block)
-        sact[r, :] = (g / (1.0 + jnp.exp(-g)) * u).astype(bf16)
-
-    @pl.loop(0, width // tile)
-    def _(i):
-        cols = pl.ds(pl.multiple_of(i * tile, tile), tile)
-        part = dot(sact[...], sdown[:, cols]).astype(bf16)
-        shared_part[:, :, cols] = part.reshape(4, block, tile)
-
-    for b in (1, 0):
-        first_copy(1, b).start()
-
-    @pl.when(owner == 1)
-    def _():
-        returned[ep] = results[ep]
+    def shared_gate_up(k):
+        g = dot(group[...], sgate[k])
+        u = dot(group[...], sup[k])
+        sact[:, k * units : (k + 1) * units] = (g / (1.0 + jnp.exp(-g)) * u).astype(bf16)
+
+    shared_gate_up(0)
 
     pieces = 4 if block % 64 == 0 else 1
     some_rows = block // pieces
-
-    for kind in range(2):
-        first_copy(kind, 1).wait_recv()
-
-        @pl.loop(0, pieces)
-        def _(i):
-            r = pl.ds(pl.multiple_of(i * some_rows, some_rows), some_rows)
-            second_out[kind, r, :] = (
-                parts[kind][far, r, :].astype(f32) + first_in[kind, 1, r, :].astype(f32)
-            ).astype(bf16)
-
-        second_copy(kind).start()
-
-    first_copy(0, 0).wait_recv()
-    second_copy(0).wait_recv()
+    first_copy(1).wait_recv()
+
+    @pl.loop(0, pieces)
+    def _(i):
+        r = pl.ds(pl.multiple_of(i * some_rows, some_rows), some_rows)
+        second_out[r, :] = (
+            mixer_part[far, r, :].astype(f32) + first_in[1, r, :].astype(f32)
+        ).astype(bf16)
+
+    second_copy.start()
+
+    for d in range(rings):
+        for j in range(3):
+            from_twin(j, d).wait_recv()
+    shared_gate_up(1)
+
+    @pl.loop(0, width // tile)
+    def _(i):
+        cols = pl.ds(pl.multiple_of(i * tile, tile), tile)
+        shared_near[:, cols] = dot(sact[near_rows, :], sdown[:, cols]).astype(bf16)
+
+    shared_copy.start()
+
+    @pl.loop(0, width // tile)
+    def _(i):
+        cols = pl.ds(pl.multiple_of(i * tile, tile), tile)
+        shared_own[:, cols] = dot(sact[own_rows, :], sdown[:, cols])
+
+    first_copy(0).wait_recv()
+    second_copy.wait_recv()
 
     @pl.loop(0, pieces)
     def _(i):
         r = pl.ds(pl.multiple_of(i * some_rows, some_rows), some_rows)
         mixer_out[r, :] = (
             mixer_part[x, r, :].astype(f32)
-            + first_in[0, 0, r, :].astype(f32)
-            + second_in[0, r, :].astype(f32)
+            + first_in[0, r, :].astype(f32)
+            + second_in[r, :].astype(f32)
         ).astype(bf16)
 
-    first_copy(1, 0).wait_recv()
-    second_copy(1).wait_recv()
+    shared_copy.wait_recv()
 
     @pl.when(owner == 1)
     def _():
@@ -515,22 +607,23 @@
     def _(i):
         cols = pl.ds(pl.multiple_of(i * tile, tile), tile)
         back = returned[:, :, cols].reshape(slots, tile)
-        total = (
-            shared_part[x, :, cols].astype(f32)
-            + first_in[1, 0, :, cols].astype(f32)
-            + second_in[1, :, cols].astype(f32)
-        )
+        total = shared_own[:, cols] + shared_in[:, cols].astype(f32)
         total = total + dot(spread_hi[...], back) + dot(spread_lo[...], back)
         expert_out[:, cols] = total.astype(bf16)
 
     for h in halos:
         h.wait_send()
-    for c in group_copies:
-        c.wait_send()
-    for kind in range(2):
-        for b in range(2):
-            first_copy(kind, b).wait_send()
-        second_copy(kind).wait_send()
+    group_copy.wait_send()
+    for b in range(2):
+        first_copy(b).wait_send()
+    second_copy.wait_send()
+    shared_copy.wait_send()
+    for j in range(3):
+        to_far_eighth(j).wait_send()
+        for d in range(rings):
+            from_ring(j, d).wait_send()
+            if d > 0:
+                round_ring(j, d).wait_send()
 
     @pl.when(owner == 1)
     def _():
@@ -575,6 +668,7 @@
     units = gate_proj.shape[2]
     capacity = 2 * block * routes.shape[1] // experts
     slots = experts * capacity
+    rings = 4 if experts % 8 == 0 else experts // 2
     tile = min(256, width)
     vmem = pl.BlockSpec(memory_space=pltpu.VMEM)
     hbm = pl.BlockSpec(memory_space=pl.ANY)
@@ -585,7 +679,7 @@
 
     out = jax.ShapeDtypeStruct((block, width), bf16)
     return pl.pallas_call(
-        functools.partial(kernel, experts, capacity, tile),
+        functools.partial(kernel, experts, capacity, rings, tile),
         name="whole",
         out_shape=(out, out),
         in_specs=[hbm, hbm, hbm, vmem, hbm, hbm, vmem] + [hbm] * 6 + [vmem, vmem],
@@ -600,7 +694,7 @@
             pltpu.VMEM((HALO + length, channels), f32),
             space(length, channels),
             space(channels, width),
-            space(4, block, width),
+            space(2 * block, width),
             space(experts, capacity, width),
             space(experts, capacity, width),
             space(experts, capacity, width),
@@ -609,24 +703,27 @@
             space(4, width, units),
             space(4, width, units),
             space(4, units, width),
-            space(width, units),
-            space(width, units),
-            space(units, width),
+            space(2, width, units),
+            space(2, width, units),
+            space(2 * units, width),
             space(slots, 4 * units),
-            space(4 * block, units),
+            space(2 * block, 2 * units),
             space(slots, block),
             space(block, slots),
             space(block, slots),
+            pltpu.VMEM((slots, width), f32),
             space(4, block, width),
-            space(4, block, width),
-            space(2, 2, block, width),
+            pltpu.VMEM((block, width), f32),
+            space(block, width),
+            space(block, width),
             space(2, block, width),
-            space(2, block, width),
+            space(block, width),
+            space(block, width),
             dma((8,)),
             dma((2,)),
             dma((2,)),
-            dma((3,)),
-            dma((3,)),
+            dma((1,)),
+            dma((1,)),
             dma((1,)),
             dma((1,)),
             dma((3,)),
@@ -634,10 +731,16 @@
             dma((6,)),
             dma((12,)),
             dma((12,)),
-            dma((4,)),
-            dma((4,)),
             dma((2,)),
             dma((2,)),
+            dma((1,)),
+            dma((1,)),
+            dma((1,)),
+            dma((1,)),
+            dma((3,)),
+            dma((3 * rings,)),
+            dma((3 * rings,)),
+            dma((6 * rings,)),
             dma((1,)),
             dma((1,)),
         ],

time: 168 us -> 149 us (0.89)
  Pallas kernels: 162 us -> 143 us
    pallas_call x1, Pallas kernels: 162 us -> 143 us  [per_device(): pl.pallas_call(functools.partial(kernel, experts, capacity, rings, tile),...]
where the time goes in v3:
time: 149 us; the launch traced here: 147 us
  Pallas kernels  143 us (96%)
  local copies, waits for them, and re-layouts  3.76 us (3%)
    pallas_call x1, Pallas kernels, per_device(): pl.pallas_call(functools.partial(kernel, experts, capacity, rings, tile),...  143 us
    unnamed x2, local copies, waits for them, and re-layouts  3.76 us

profile of v3, /device:TPU:1, one launch (start us, length us, event | category | flops | bytes accessed | tf_op | source)
XLA Modules:
  0.0 147.4 jit_solution(15960665954242448466)
XLA Ops:
  0.6 142.9 %whole.1 = (bf16[128,2048]{1,0:T(8,128)(2,1)}, bf16[128,2048]{1,0:T(8,128)(2,1)}) custom-call(bf16[512,512]{1,0:T(8,128)(2,1)} %outer_hbm.1, bf16[512,512]{1,0:T(8,128)(2,1)} %inner_hbm.1, bf16[512,512]{1,0:T(8,128)(2,1)} %values_hbm.1, bf16[3,512]{1,0:T(4,128)(2,1)} %taps.1, bf16[512,2048]{1,0:T(8,128)(2,1)} %outw_hbm.1, bf16[128,2048]{1,0:T(8,128)(2,1)} %moe_hbm.1, ...), custom_call_target="tpu_custom_call" | custom-call | tf_op jit(solution)/shard_map/whole/pallas_call | solution.py:681
  143.6 1.9 %copy.19 = bf16[128,2048]{1,0:T(8,128)(2,1)} copy(bf16[128,2048]{1,0:T(8,128)(2,1)} %get-tuple-element.4) | data formatting | bytes 1048576
  145.5 1.9 %copy.20 = bf16[128,2048]{1,0:T(8,128)(2,1)} copy(bf16[128,2048]{1,0:T(8,128)(2,1)} %get-tuple-element.5) | data formatting | bytes 1048576

commit v4 on v3

--- a/solution.py
+++ b/solution.py
@@ -12,6 +12,7 @@
 bf16 = jnp.bfloat16
 f32 = jnp.float32
 HALO = 16
+PIECES = 6
 
 
 def remote(src, dst, send_sem, recv_sem, ep, tp):
@@ -33,6 +34,7 @@
     experts,
     capacity,
     rings,
+    layers,
     tile,
     outer_hbm,
     inner_hbm,
@@ -104,6 +106,8 @@
     shared_send,
     shared_recv,
     eighth_send,
+    layer_send,
+    layer_recv,
     ring_send,
     pass_send,
     eighth_recv,
@@ -125,6 +129,8 @@
     units = sgate.shape[2]
     own_rows, near_rows = pl.ds(0, block), pl.ds(block, block)
     y = lax.rem(chip, rings)
+    z = lax.div(chip, rings)
+    layer = lax.rem(z, layers)
     eighths = 2 * rings
     eighth = 2 * y + core
     slots = experts * capacity
@@ -142,30 +148,36 @@
     loads = [pltpu.make_async_copy(s, d, load_sem.at[i]) for i, (s, d) in enumerate(loads)]
     loads[0].start()
 
-    own_pieces = [gate_hbm.at[0], up_hbm.at[0], down_hbm.at[0]]
-    held = [wgate, wup, wdown]
+    quarter = units // 4
+
+    def own_piece(j):
+        if j < 2:
+            return [gate_hbm, up_hbm][j].at[0]
+        return down_hbm.at[0, pl.ds((j - 2) * quarter, quarter)]
+
+    def held_piece(k, j):
+        if j < 2:
+            return [wgate, wup][j].at[k]
+        return wdown.at[k, pl.ds((j - 2) * quarter, quarter)]
+
+    def weight_copy(src, k, j, send, device, tp):
+        return remote(src, held_piece(k, j), send, weight_recv.at[PIECES * k + j], device, tp)
 
     def to_near(j):
-        return remote(
-            own_pieces[j], held[j].at[1], near_send.at[j], weight_recv.at[3 + j], ep, near
-        )
+        return weight_copy(own_piece(j), 1, j, near_send.at[j], ep, near)
 
     def to_far(j):
-        return remote(own_pieces[j], held[j].at[2], far_send.at[j], weight_recv.at[6 + j], ep, far)
+        return weight_copy(own_piece(j), 2, j, far_send.at[j], ep, far)
 
     def onward(j):
-        return remote(
-            held[j].at[2], held[j].at[3], near_send.at[3 + j], weight_recv.at[9 + j], ep, near
-        )
+        return weight_copy(held_piece(2, j), 3, j, near_send.at[PIECES + j], ep, near)
 
     def to_twin(k, j):
-        source = own_pieces[j] if k == 0 else held[j].at[k]
-        return remote(
-            source, held[j].at[k], twin_send.at[3 * k + j], weight_recv.at[3 * k + j], twin, x
-        )
+        source = own_piece(j) if k == 0 else held_piece(k, j)
+        return weight_copy(source, k, j, twin_send.at[PIECES * k + j], twin, x)
 
     def keep_own(j):
-        return pltpu.make_async_copy(own_pieces[j], held[j].at[0], own_sem.at[j])
+        return pltpu.make_async_copy(own_piece(j), held_piece(0, j), own_sem.at[j])
 
     barrier = pltpu.get_barrier_semaphore()
 
@@ -179,8 +191,11 @@
     greet(lax.rem(ep + experts - 1, experts), x)
 
     greet(twin, x)
-    for d in range(1, rings):
+    sides = [1, rings - 1] if rings > 2 else [1]
+    for d in sides:
         greet(2 * (chip - y + lax.rem(y + d, rings)) + core, x)
+    for d in range(1, layers):
+        greet(2 * ((z - layer + lax.rem(layer + d, layers)) * rings + y) + core, x)
 
     @pl.loop(0, experts)
     def _(i):
@@ -192,7 +207,7 @@
 
     @pl.when(owner == 1)
     def _():
-        for j in range(3):
+        for j in range(PIECES):
             keep_own(j).start()
 
     for c in loads[1:]:
@@ -250,17 +265,9 @@
             x + (far - x) * cross,
         )
 
-    pl.semaphore_wait(barrier, experts + 3 + rings - owner)
+    pl.semaphore_wait(barrier, experts + 3 + len(sides) + layers - owner)
     for h in halos:
         h.start()
-
-    @pl.loop(0, experts)
-    def _(i):
-        e = lax.rem(ep + 1 + i, experts)
-
-        @pl.when(e != own_index)
-        def _():
-            send_out(e).start()
 
     shared_hbm = [sgate_hbm, sup_hbm, sdown_hbm]
 
@@ -270,16 +277,50 @@
             return [sgate, sup][j].at[1, pl.ds(pl.multiple_of(i * n, n), n)]
         return sdown.at[pl.ds(pl.multiple_of(units + i * n, n), n)]
 
-    def to_far_eighth(j):
-        n = shared_hbm[j].shape[0] // eighths
-        return remote(
-            shared_hbm[j].at[pl.ds(pl.multiple_of(eighth * n, n), n)],
-            held_eighth(j, eighth),
+    def held_layer(j, at_layer):
+        n = shared_hbm[j].shape[0] // (eighths * layers)
+        first = pl.multiple_of((eighth * layers + at_layer) * n, n)
+        if j < 2:
+            return [sgate, sup][j].at[1, pl.ds(first, n)]
+        return sdown.at[pl.ds(pl.multiple_of(units + first, n), n)]
+
+    def to_far_layer(j):
+        n = shared_hbm[j].shape[0] // (eighths * layers)
+        first = pl.multiple_of((eighth * layers + layer) * n, n)
+        return remote(
+            shared_hbm[j].at[pl.ds(first, n)],
+            held_layer(j, layer),
             eighth_send.at[j],
-            eighth_recv.at[3 * eighth + j],
+            layer_recv.at[3 * layer + j],
             ep,
             far,
         )
+
+    def layer_device(d):
+        return 2 * ((z - layer + lax.rem(layer + d, layers)) * rings + y) + core
+
+    def to_layer(j, d):
+        return remote(
+            held_layer(j, layer),
+            held_layer(j, layer),
+            layer_send.at[3 * d + j],
+            layer_recv.at[3 * layer + j],
+            layer_device(d),
+            x,
+        )
+
+    def from_layer(j, d):
+        source = lax.rem(layer + d, layers)
+        return remote(
+            held_layer(j, source),
+            held_layer(j, source),
+            layer_send.at[3 * d + j],
+            layer_recv.at[3 * source + j],
+            layer_device(d),
+            x,
+        )
+
+    tiles = width // tile // 2
 
     def round_ring(j, d):
         return remote(
@@ -291,6 +332,18 @@
             x,
         )
 
+    def opposite(j):
+        d = 1 if j == 1 else rings - 1
+        i = 2 * lax.rem(y + d, rings) + core
+        return remote(
+            held_eighth(j, i),
+            held_eighth(j, i),
+            ring_send.at[j],
+            eighth_recv.at[3 * i + j],
+            2 * (chip - y + lax.rem(y + rings - d, rings)) + core,
+            x,
+        )
+
     def from_ring(j, d):
         i = 2 * lax.rem(y + d, rings) + core
         return remote(
@@ -313,19 +366,28 @@
             x,
         )
 
+    for j in range(3):
+        to_far_layer(j).start()
+
+    @pl.loop(0, experts)
+    def _(i):
+        e = lax.rem(ep + 1 + i, experts)
+
+        @pl.when(e != own_index)
+        def _():
+            send_out(e).start()
+
     @pl.when(owner == 1)
     def _():
-        for j in range(3):
+        for j in range(PIECES):
             to_near(j).start()
-        for j in range(3):
+        for j in range(PIECES):
             to_twin(0, j).start()
 
     @pl.when(owner == 0)
     def _():
-        for j in range(3):
+        for j in range(PIECES):
             to_far(j).start()
-        for j in range(3):
-            to_far_eighth(j).start()
 
     def relay(j):
         @pl.when(owner == 1)
@@ -333,6 +395,10 @@
             to_far(j).wait_recv()
             onward(j).start()
             to_twin(2, j).start()
+
+    def pass_near(j):
+        @pl.when(owner == 1)
+        def _():
             to_near(j).wait_recv()
             to_twin(1, j).start()
 
@@ -376,13 +442,32 @@
     @pl.loop(0, width // tile)
     def _(i):
         cols = pl.ds(pl.multiple_of(i * tile, tile), tile)
+        some = pl.ds(pl.multiple_of(lax.rem(i, tiles) * tile, tile), tile)
         part = dot(gated[...], outw[:, cols]).astype(bf16)
-        mixer_part[:, :, cols] = part.reshape(4, block, tile)
-
+        mixer_part[lax.div(i, tiles), :, :, some] = part.reshape(4, block, tile)
+
+    for j in range(3):
+        to_far_layer(j).wait_recv()
+        for d in range(1, layers):
+            to_layer(j, d).start()
+    pass_near(0)
+    pass_near(1)
     relay(0)
+    for j in range(2, PIECES):
+        pass_near(j)
 
     relay(1)
     relay(2)
+    relay(3)
+
+    for j in range(3):
+        for d in range(1, layers):
+            from_layer(j, d).wait_recv()
+        for d in sides:
+            round_ring(j, d).start()
+        from_ring(j, 0).start()
+    relay(4)
+    relay(5)
 
     def passed(j):
         @pl.when(owner == 1)
@@ -390,11 +475,6 @@
             onward(j).wait_recv()
             to_twin(3, j).start()
 
-    @pl.when(owner == 1)
-    def _():
-        for j in range(3):
-            to_far_eighth(j).start()
-
     passed(0)
 
 
@@ -408,6 +488,7 @@
         remote(landed, landed, out_send.at[0], out_recv.at[0], twin, x).wait_recv()
 
     half = slots // 2
+    half_experts = experts // 2
 
     @pl.loop(0, width // tile)
     def _(i):
@@ -445,11 +526,13 @@
     @pl.when(owner == 0)
     def _():
         for k in range(3):
-            to_twin(k, 2).wait_recv()
+            for j in range(2, PIECES):
+                to_twin(k, j).wait_recv()
 
     @pl.when(owner == 1)
     def _():
-        keep_own(2).wait()
+        for j in range(2, PIECES):
+            keep_own(j).wait()
 
     @pl.loop(0, width // tile)
     def _(i):
@@ -461,6 +544,14 @@
                 total = total + dot(act[r, k * units : (k + 1) * units], wdown[k, :, cols])
             total_down[r, cols] = total
 
+    for j in range(3):
+        for d in sides:
+            from_ring(j, d).wait_recv()
+        if rings > 2:
+            opposite(j).start()
+        for d in sides:
+            from_ring(j, d).start()
+
     for j in range(2):
 
         @pl.when(owner == 0)
@@ -473,68 +564,78 @@
         group.at[own_rows], group.at[near_rows], group_send.at[0], group_recv.at[0], ep, near
     )
 
-    def first_copy(b):
-        src = near if b == 0 else 3 - near
-        return remote(
-            mixer_part.at[src], first_in.at[b], first_send.at[b], first_recv.at[b], ep, near
-        )
-
-    second_copy = remote(
-        second_out, second_in, second_send.at[0], second_recv.at[0], ep, far
-    )
+    partners = [near, far]
+
+    def first_copy(h, b):
+        src = partners[h] if b == 0 else 3 - near
+        return remote(
+            mixer_part.at[h, src],
+            first_in.at[h, b],
+            first_send.at[2 * h + b],
+            first_recv.at[2 * h + b],
+            ep,
+            partners[h],
+        )
+
+    def second_copy(h):
+        return remote(
+            second_out.at[h],
+            second_in.at[h],
+            second_send.at[h],
+            second_recv.at[h],
+            ep,
+            partners[1 - h],
+        )
+
     shared_copy = remote(
         shared_near, shared_in, shared_send.at[0], shared_recv.at[0], ep, near
     )
 
+    for j in range(2, PIECES):
+        passed(j)
+
+    @pl.when(owner == 0)
+    def _():
+        for j in range(2, PIECES):
+            to_twin(3, j).wait_recv()
+
     group_copy.start()
     for b in (1, 0):
-        first_copy(b).start()
-
-    for j in range(3):
-        to_far_eighth(j).wait_recv()
-        for d in range(1, rings):
-            round_ring(j, d).start()
-        from_ring(j, 0).start()
-
-    passed(2)
-
-    @pl.when(owner == 0)
-    def _():
-        to_twin(3, 2).wait_recv()
+        first_copy(0, b).start()
 
     def send_back(s):
         return remote(
             results.at[s], returned.at[mine], back_send.at[0], back_recv.at[0], s, plane
         )
 
-    chunks = 4 if slots % 64 == 0 and experts % 4 == 0 else 1
-    chunk, chunk_experts = slots // chunks, experts // chunks
-
-    @pl.loop(0, chunks)
-    def _(m):
-        r = pl.ds(pl.multiple_of(m * chunk, chunk), chunk)
-
-        @pl.loop(0, width // tile)
+    def down(m):
+        r = pl.ds(m * half, half)
+        e = pl.ds(m * half_experts, half_experts)
+        for i in range(width // tile):
+            cols = pl.ds(i * tile, tile)
+            total = total_down[r, cols] + dot(act[r, 3 * units : 4 * units], wdown[3, :, cols])
+            results[e, :, cols] = total.reshape(half_experts, capacity, tile).astype(bf16)
+
+        @pl.loop(0, half_experts)
         def _(i):
-            cols = pl.ds(pl.multiple_of(i * tile, tile), tile)
-            total = total_down[r, cols] + dot(act[r, 3 * units : 4 * units], wdown[3, :, cols])
-            results[pl.ds(m * chunk_experts, chunk_experts), :, cols] = total.reshape(
-                chunk_experts, capacity, tile
-            ).astype(bf16)
-
-        @pl.loop(0, chunk_experts)
-        def _(i):
-            s = m * chunk_experts + lax.rem(ep + 1 + i, chunk_experts)
+            s = m * half_experts + lax.rem(ep + 1 + i, half_experts)
 
             @pl.when(s != own_index)
             def _():
                 send_back(s).start()
 
+    down(0)
+
+    down(1)
+
+    for b in (1, 0):
+        first_copy(1, b).start()
+
     @pl.when(owner == 1)
     def _():
         returned[ep] = results[ep]
 
-    for d in range(1, rings):
+    for d in range(2, rings - 1):
         for j in range(3):
             from_ring(j, d).wait_recv()
             from_ring(j, d).start()
@@ -552,45 +653,50 @@
 
     pieces = 4 if block % 64 == 0 else 1
     some_rows = block // pieces
-    first_copy(1).wait_recv()
-
-    @pl.loop(0, pieces)
-    def _(i):
-        r = pl.ds(pl.multiple_of(i * some_rows, some_rows), some_rows)
-        second_out[r, :] = (
-            mixer_part[far, r, :].astype(f32) + first_in[1, r, :].astype(f32)
-        ).astype(bf16)
-
-    second_copy.start()
+
+    def pass_sum(h):
+        first_copy(h, 1).wait_recv()
+
+        @pl.loop(0, pieces)
+        def _(i):
+            r = pl.ds(pl.multiple_of(i * some_rows, some_rows), some_rows)
+            second_out[h, r, :] = (
+                mixer_part[h, partners[1 - h], r, :].astype(f32)
+                + first_in[h, 1, r, :].astype(f32)
+            ).astype(bf16)
+
+        second_copy(h).start()
 
     for d in range(rings):
         for j in range(3):
             from_twin(j, d).wait_recv()
     shared_gate_up(1)
 
-    @pl.loop(0, width // tile)
-    def _(i):
-        cols = pl.ds(pl.multiple_of(i * tile, tile), tile)
+    for i in range(width // tile):
+        cols = pl.ds(i * tile, tile)
         shared_near[:, cols] = dot(sact[near_rows, :], sdown[:, cols]).astype(bf16)
 
     shared_copy.start()
 
-    @pl.loop(0, width // tile)
-    def _(i):
-        cols = pl.ds(pl.multiple_of(i * tile, tile), tile)
+    for i in range(width // tile):
+        cols = pl.ds(i * tile, tile)
         shared_own[:, cols] = dot(sact[own_rows, :], sdown[:, cols])
 
-    first_copy(0).wait_recv()
-    second_copy.wait_recv()
-
-    @pl.loop(0, pieces)
-    def _(i):
-        r = pl.ds(pl.multiple_of(i * some_rows, some_rows), some_rows)
-        mixer_out[r, :] = (
-            mixer_part[x, r, :].astype(f32)
-            + first_in[0, r, :].astype(f32)
-            + second_in[r, :].astype(f32)
-        ).astype(bf16)
+    pass_sum(0)
+    pass_sum(1)
+
+    for h in range(2):
+        first_copy(h, 0).wait_recv()
+        second_copy(h).wait_recv()
+
+        @pl.loop(0, pieces)
+        def _(i):
+            r = pl.ds(pl.multiple_of(i * some_rows, some_rows), some_rows)
+            mixer_out[r, h * (width // 2) : (h + 1) * (width // 2)] = (
+                mixer_part[h, x, r, :].astype(f32)
+                + first_in[h, 0, r, :].astype(f32)
+                + second_in[h, r, :].astype(f32)
+            ).astype(bf16)
 
     shared_copy.wait_recv()
 
@@ -603,9 +709,8 @@
     def _():
         remote(returned, returned, back_send.at[0], back_recv.at[0], twin, x).wait_recv()
 
-    @pl.loop(0, width // tile)
-    def _(i):
-        cols = pl.ds(pl.multiple_of(i * tile, tile), tile)
+    for i in range(width // tile):
+        cols = pl.ds(i * tile, tile)
         back = returned[:, :, cols].reshape(slots, tile)
         total = shared_own[:, cols] + shared_in[:, cols].astype(f32)
         total = total + dot(spread_hi[...], back) + dot(spread_lo[...], back)
@@ -614,20 +719,25 @@
     for h in halos:
         h.wait_send()
     group_copy.wait_send()
-    for b in range(2):
-        first_copy(b).wait_send()
-    second_copy.wait_send()
+    for h in range(2):
+        for b in range(2):
+            first_copy(h, b).wait_send()
+        second_copy(h).wait_send()
     shared_copy.wait_send()
     for j in range(3):
-        to_far_eighth(j).wait_send()
+        to_far_layer(j).wait_send()
+        for d in range(1, layers):
+            to_layer(j, d).wait_send()
         for d in range(rings):
             from_ring(j, d).wait_send()
-            if d > 0:
-                round_ring(j, d).wait_send()
+        for d in sides:
+            round_ring(j, d).wait_send()
+        if rings > 2:
+            opposite(j).wait_send()
 
     @pl.when(owner == 1)
     def _():
-        for j in range(3):
+        for j in range(PIECES):
             to_near(j).wait_send()
             onward(j).wait_send()
             for k in range(4):
@@ -639,7 +749,7 @@
 
     @pl.when(owner == 0)
     def _():
-        for j in range(3):
+        for j in range(PIECES):
             to_far(j).wait_send()
         remote(outgoing, outgoing, out_send.at[0], out_recv.at[0], twin, x).wait_send()
         remote(results, results, back_send.at[0], back_recv.at[0], twin, x).wait_send()
@@ -668,7 +778,8 @@
     units = gate_proj.shape[2]
     capacity = 2 * block * routes.shape[1] // experts
     slots = experts * capacity
-    rings = 4 if experts % 8 == 0 else experts // 2
+    rings = 4 if experts % 32 == 0 else 2
+    layers = min(4, experts // (2 * rings))
     tile = min(256, width)
     vmem = pl.BlockSpec(memory_space=pltpu.VMEM)
     hbm = pl.BlockSpec(memory_space=pl.ANY)
@@ -679,7 +790,7 @@
 
     out = jax.ShapeDtypeStruct((block, width), bf16)
     return pl.pallas_call(
-        functools.partial(kernel, experts, capacity, rings, tile),
+        functools.partial(kernel, experts, capacity, rings, layers, tile),
         name="whole",
         out_shape=(out, out),
         in_specs=[hbm, hbm, hbm, vmem, hbm, hbm, vmem] + [hbm] * 6 + [vmem, vmem],
@@ -712,13 +823,13 @@
             space(block, slots),
             space(block, slots),
             pltpu.VMEM((slots, width), f32),
-            space(4, block, width),
+            space(2, 4, block, width // 2),
             pltpu.VMEM((block, width), f32),
             space(block, width),
             space(block, width),
-            space(2, block, width),
-            space(block, width),
-            space(block, width),
+            space(2, 2, block, width // 2),
+            space(2, block, width // 2),
+            space(2, block, width // 2),
             dma((8,)),
             dma((2,)),
             dma((2,)),
@@ -726,18 +837,20 @@
             dma((1,)),
             dma((1,)),
             dma((1,)),
-            dma((3,)),
-            dma((3,)),
-            dma((6,)),
-            dma((12,)),
-            dma((12,)),
+            dma((PIECES,)),
+            dma((PIECES,)),
+            dma((2 * PIECES,)),
+            dma((4 * PIECES,)),
+            dma((4 * PIECES,)),
+            dma((4,)),
+            dma((4,)),
             dma((2,)),
             dma((2,)),
             dma((1,)),
             dma((1,)),
-            dma((1,)),
-            dma((1,)),
             dma((3,)),
+            dma((3 * layers,)),
+            dma((3 * layers,)),
             dma((3 * rings,)),
             dma((3 * rings,)),
             dma((6 * rings,)),

time: 149 us -> 146 us (0.980)
  the two profiles are of different devices: /device:TPU:1 before, /device:TPU:179 now
where the time goes in v4:
time: 146 us
  Pallas kernels  142 us (97%)
  local copies, waits for them, and re-layouts  3.76 us (3%)
    pallas_call x1, Pallas kernels, per_device(): pl.pallas_call(functools.partial(kernel, experts, capacity, rings, layers...  142 us
    unnamed x2, local copies, waits for them, and re-layouts  3.76 us

profile of v4, /device:TPU:179, one launch (start us, length us, event | category | flops | bytes accessed | tf_op | source)
XLA Modules:
  0.0 146.2 jit_solution(7574656182363711282)
XLA Ops:
  0.6 141.8 %whole.1 = (bf16[128,2048]{1,0:T(8,128)(2,1)}, bf16[128,2048]{1,0:T(8,128)(2,1)}) custom-call(bf16[512,512]{1,0:T(8,128)(2,1)} %outer_hbm.1, bf16[512,512]{1,0:T(8,128)(2,1)} %inner_hbm.1, bf16[512,512]{1,0:T(8,128)(2,1)} %values_hbm.1, bf16[3,512]{1,0:T(4,128)(2,1)} %taps.1, bf16[512,2048]{1,0:T(8,128)(2,1)} %outw_hbm.1, bf16[128,2048]{1,0:T(8,128)(2,1)} %moe_hbm.1, ...), custom_call_target="tpu_custom_call" | custom-call | tf_op jit(solution)/shard_map/whole/pallas_call | solution.py:792
  142.4 1.9 %copy.19 = bf16[128,2048]{1,0:T(8,128)(2,1)} copy(bf16[128,2048]{1,0:T(8,128)(2,1)} %get-tuple-element.4) | data formatting | bytes 1048576
  144.3 1.9 %copy.20 = bf16[128,2048]{1,0:T(8,128)(2,1)} copy(bf16[128,2048]{1,0:T(8,128)(2,1)} %get-tuple-element.5) | data formatting | bytes 1048576

commit v5 on v4

--- a/solution.py
+++ b/solution.py
@@ -254,6 +254,12 @@
         taken = dot(pick[...], group[own_rows, cols])
         outgoing[:, :, cols] = taken.reshape(experts, capacity, tile).astype(bf16)
 
+    def spread_order(i):
+        per = min(8, experts)
+        deep = experts // per
+        dz, dw = lax.rem(3 * lax.rem(i, deep), deep), lax.div(i, deep)
+        return lax.rem(lax.div(ep, per) + dz, deep) * per + lax.rem(ep + dw, per)
+
     def send_out(e):
         cross = lax.rem(lax.rem(e, 2) + side, 2)
         return remote(
@@ -371,7 +377,7 @@
 
     @pl.loop(0, experts)
     def _(i):
-        e = lax.rem(ep + 1 + i, experts)
+        e = spread_order(i)
 
         @pl.when(e != own_index)
         def _():
@@ -616,17 +622,16 @@
             total = total_down[r, cols] + dot(act[r, 3 * units : 4 * units], wdown[3, :, cols])
             results[e, :, cols] = total.reshape(half_experts, capacity, tile).astype(bf16)
 
-        @pl.loop(0, half_experts)
-        def _(i):
-            s = m * half_experts + lax.rem(ep + 1 + i, half_experts)
-
-            @pl.when(s != own_index)
-            def _():
-                send_back(s).start()
-
     down(0)
-
     down(1)
+
+    @pl.loop(0, experts)
+    def _(i):
+        s = spread_order(i)
+
+        @pl.when(s != own_index)
+        def _():
+            send_back(s).start()
 
     for b in (1, 0):
         first_copy(1, b).start()
@@ -753,6 +758,24 @@
             to_far(j).wait_send()
         remote(outgoing, outgoing, out_send.at[0], out_recv.at[0], twin, x).wait_send()
         remote(results, results, back_send.at[0], back_recv.at[0], twin, x).wait_send()
+
+
+def leave(mixer_in, expert_in, mixer_out, expert_out, mixer, expert, in_sem, out_sem):
+    ins = [
+        pltpu.make_async_copy(mixer_in, mixer, in_sem.at[0]),
+        pltpu.make_async_copy(expert_in, expert, in_sem.at[1]),
+    ]
+    outs = [
+        pltpu.make_async_copy(mixer, mixer_out, out_sem.at[0]),
+        pltpu.make_async_copy(expert, expert_out, out_sem.at[1]),
+    ]
+    for c in ins:
+        c.start()
+    for i, o in zip(ins, outs):
+        i.wait()
+        o.start()
+    for c in outs:
+        c.wait()
 
 
 def per_device(
@@ -789,7 +812,7 @@
         return pltpu.VMEM(shape, bf16)
 
     out = jax.ShapeDtypeStruct((block, width), bf16)
-    return pl.pallas_call(
+    outs = pl.pallas_call(
         functools.partial(kernel, experts, capacity, rings, layers, tile),
         name="whole",
         out_shape=(out, out),
@@ -877,6 +900,14 @@
         routes.T,
         route_weight.T,
     )
+    return pl.pallas_call(
+        leave,
+        name="leave",
+        out_shape=(out, out),
+        in_specs=[hbm, hbm],
+        out_specs=(hbm, hbm),
+        scratch_shapes=[space(block, width), space(block, width), dma((2,)), dma((2,))],
+    )(*outs)
 
 
 def solution(mesh):

time: 146 us -> 142 us (0.973)
  the two profiles are of different devices: /device:TPU:179 before, /device:TPU:1 now
where the time goes in v5:
time: 142 us
  Pallas kernels  141 us (99%)
    pallas_call x1, Pallas kernels, per_device(): pl.pallas_call(functools.partial(kernel, experts, capacity, rings, layers...  139 us

profile of v5, /device:TPU:1, one launch (start us, length us, event | category | flops | bytes accessed | tf_op | source)
XLA Modules:
  0.0 141.7 jit_solution(17312683337094855398)
XLA Ops:
  0.6 139.0 %whole.1 = (bf16[128,2048]{1,0:T(8,128)(2,1)}, bf16[128,2048]{1,0:T(8,128)(2,1)}) custom-call(bf16[512,512]{1,0:T(8,128)(2,1)} %outer_hbm.1, bf16[512,512]{1,0:T(8,128)(2,1)} %inner_hbm.1, bf16[512,512]{1,0:T(8,128)(2,1)} %values_hbm.1, bf16[3,512]{1,0:T(4,128)(2,1)} %taps.1, bf16[512,2048]{1,0:T(8,128)(2,1)} %outw_hbm.1, bf16[128,2048]{1,0:T(8,128)(2,1)} %moe_hbm.1, ...), custom_call_target="tpu_custom_call" | custom-call | tf_op jit(solution)/shard_map/whole/pallas_call | solution.py:815
  139.6 2.0 %leave.1 = (bf16[128,2048]{1,0:T(8,128)(2,1)}, bf16[128,2048]{1,0:T(8,128)(2,1)}) custom-call(bf16[128,2048]{1,0:T(8,128)(2,1)} %get-tuple-element.4.mixer_in, bf16[128,2048]{1,0:T(8,128)(2,1)} %get-tuple-element.5.expert_in), custom_call_target="tpu_custom_call" | custom-call | tf_op jit(solution)/shard_map/leave/pallas_call | solution.py:903

commit v6 on v5

--- a/solution.py
+++ b/solution.py
@@ -113,6 +113,7 @@
     eighth_recv,
     back_send,
     back_recv,
+    met,
 ):
     ep, x = lax.axis_index("ep"), lax.axis_index("tp")
     core, chip = lax.rem(ep, 2), lax.div(ep, 2)
@@ -120,7 +121,6 @@
     far = 3 - x
     side = lax.div(x, 2)
     owner = 1 - lax.rem(core + side, 2)
-    own_index = ep * owner - (1 - owner)
     twin = ep + 1 - 2 * core
     plane = x + (far - x) * (1 - owner)
     mine = 2 * chip + side
@@ -188,22 +188,35 @@
 
     greet(ep, near)
     greet(ep, far)
-    greet(lax.rem(ep + experts - 1, experts), x)
-
     greet(twin, x)
     sides = [1, rings - 1] if rings > 2 else [1]
+    deep = experts // (2 * rings)
+
+    def along_y(d):
+        return 2 * (chip - y + lax.rem(y + d, rings)) + core
+
+    def along_z(d):
+        return ep + 2 * rings * d
+
+    def below(d):
+        return lax.div(z + deep - d, deep)
+
+    def above(d):
+        return lax.div(2 * deep - 1 - z - d, deep)
+
     for d in sides:
-        greet(2 * (chip - y + lax.rem(y + d, rings)) + core, x)
-    for d in range(1, layers):
-        greet(2 * ((z - layer + lax.rem(layer + d, layers)) * rings + y) + core, x)
-
-    @pl.loop(0, experts)
-    def _(i):
-        s = lax.rem(ep + 1 + i, experts)
-
-        @pl.when(s != own_index)
+        greet(along_y(d), x)
+
+    def tell_z(d, tell):
+        @pl.when(below(d) == 1)
         def _():
-            greet(s, plane)
+            tell(along_z(-d), x)
+
+        @pl.when(above(d) == 1)
+        def _():
+            tell(along_z(d), x)
+
+    tell_z(1, greet)
 
     @pl.when(owner == 1)
     def _():
@@ -219,6 +232,146 @@
         remote(inner_hbm.at[tail], halo_inner, halo_send.at[0], halo_recv.at[0], after, x),
         remote(values_hbm.at[tail], halo_values, halo_send.at[1], halo_recv.at[1], after, x),
     ]
+
+    shared_hbm = [sgate_hbm, sup_hbm, sdown_hbm]
+
+    def held_eighth(j, i):
+        n = shared_hbm[j].shape[0] // eighths
+        if j < 2:
+            return [sgate, sup][j].at[1, pl.ds(pl.multiple_of(i * n, n), n)]
+        return sdown.at[pl.ds(pl.multiple_of(units + i * n, n), n)]
+
+    def held_layer(j, at_layer):
+        n = shared_hbm[j].shape[0] // (eighths * layers)
+        first = pl.multiple_of((eighth * layers + at_layer) * n, n)
+        if j < 2:
+            return [sgate, sup][j].at[1, pl.ds(first, n)]
+        return sdown.at[pl.ds(pl.multiple_of(units + first, n), n)]
+
+    def to_far_layer(j):
+        n = shared_hbm[j].shape[0] // (eighths * layers)
+        first = pl.multiple_of((eighth * layers + layer) * n, n)
+        return remote(
+            shared_hbm[j].at[pl.ds(first, n)],
+            held_layer(j, layer),
+            eighth_send.at[j],
+            layer_recv.at[3 * layer + j],
+            ep,
+            far,
+        )
+
+    def layer_device(d):
+        return 2 * ((z - layer + lax.rem(layer + d, layers)) * rings + y) + core
+
+    def to_layer(j, d):
+        return remote(
+            held_layer(j, layer),
+            held_layer(j, layer),
+            layer_send.at[3 * d + j],
+            layer_recv.at[3 * layer + j],
+            layer_device(d),
+            x,
+        )
+
+    def from_layer(j, d):
+        source = lax.rem(layer + d, layers)
+        return remote(
+            held_layer(j, source),
+            held_layer(j, source),
+            layer_send.at[3 * d + j],
+            layer_recv.at[3 * source + j],
+            layer_device(d),
+            x,
+        )
+
+    tiles = width // tile // 2
+
+    def round_ring(j, d):
+        return remote(
+            held_eighth(j, eighth),
+            held_eighth(j, eighth),
+            ring_send.at[3 * d + j],
+            eighth_recv.at[3 * eighth + j],
+            2 * (chip - y + lax.rem(y + d, rings)) + core,
+            x,
+        )
+
+    def opposite(j):
+        d = 1 if j == 1 else rings - 1
+        i = 2 * lax.rem(y + d, rings) + core
+        return remote(
+            held_eighth(j, i),
+            held_eighth(j, i),
+            ring_send.at[j],
+            eighth_recv.at[3 * i + j],
+            2 * (chip - y + lax.rem(y + rings - d, rings)) + core,
+            x,
+        )
+
+    def from_ring(j, d):
+        i = 2 * lax.rem(y + d, rings) + core
+        return remote(
+            held_eighth(j, i),
+            held_eighth(j, i),
+            pass_send.at[3 * d + j],
+            eighth_recv.at[3 * i + j],
+            twin,
+            x,
+        )
+
+    def from_twin(j, d):
+        i = 2 * lax.rem(y + d, rings) + 1 - core
+        return remote(
+            held_eighth(j, i),
+            held_eighth(j, i),
+            pass_send.at[3 * d + j],
+            eighth_recv.at[3 * i + j],
+            twin,
+            x,
+        )
+
+    pl.semaphore_wait(barrier, 3 + len(sides) + below(1) + above(1))
+    for j in range(3):
+        to_far_layer(j).start()
+
+    @pl.when(owner == 1)
+    def _():
+        for j in range(PIECES):
+            to_near(j).start()
+        for j in range(PIECES):
+            to_twin(0, j).start()
+
+    @pl.when(owner == 0)
+    def _():
+        to_far(0).start()
+
+    stages = [None] + [sides] * (2 if rings > 2 else 1)
+    stages += [d for d in (1, 2, 4) if d < deep]
+
+    def announce(n):
+        def tell(device, tp):
+            pl.semaphore_signal(
+                met.at[n], inc=1, device_id={"ep": device, "tp": tp}, device_id_type=MESH
+            )
+
+        if n == 0:
+            tell(twin, x)
+        elif isinstance(stages[n], list):
+            for d in stages[n]:
+                tell(along_y(d), x)
+        else:
+            tell_z(stages[n], tell)
+
+    def meet(n):
+        if n == 0:
+            count = 1
+        elif isinstance(stages[n], list):
+            count = len(stages[n])
+        else:
+            count = below(stages[n]) + above(stages[n])
+        pl.semaphore_wait(met.at[n], count)
+
+    announce(0)
 
     at = pl.ds(pl.multiple_of(x * block, block), block)
     chosen = [routes[k : k + 1, at].astype(f32) for k in range(2)]
@@ -237,6 +390,9 @@
         bf16
     )
 
+    meet(0)
+    announce(1)
+
     loads[0].wait()
     scale = gain[...].reshape(1, width).astype(f32)
     step = min(16, block)
@@ -248,6 +404,10 @@
         square = jnp.mean(v * v, axis=-1, keepdims=True)
         group[r, :] = (v * lax.rsqrt(square + epsilon) * scale).astype(bf16)
 
+    meet(1)
+    if len(stages) > 2:
+        announce(2)
+
     @pl.loop(0, width // tile)
     def _(i):
         cols = pl.ds(pl.multiple_of(i * tile, tile), tile)
@@ -260,139 +420,50 @@
         dz, dw = lax.rem(3 * lax.rem(i, deep), deep), lax.div(i, deep)
         return lax.rem(lax.div(ep, per) + dz, deep) * per + lax.rem(ep + dw, per)
 
-    def send_out(e):
+    def source_order(i):
+        per = min(8, experts)
+        deep = experts // per
+        dz, dw = lax.rem(3 * lax.rem(i, deep), deep), lax.div(i, deep)
+        return lax.rem(lax.div(mine, per) + deep - dz, deep) * per + lax.rem(
+            lax.rem(mine, per) + per - dw, per
+        )
+
+    half = slots // 2
+    half_experts = experts // 2
+
+    def send_out(i):
+        e = spread_order(i)
         cross = lax.rem(lax.rem(e, 2) + side, 2)
         return remote(
             outgoing.at[e],
-            landed.at[ep],
+            landed.at[i],
             out_send.at[0],
-            out_recv.at[0],
+            out_recv.at[lax.div(i, half_experts)],
             2 * lax.div(e, 2) + side,
             x + (far - x) * cross,
         )
 
-    pl.semaphore_wait(barrier, experts + 3 + len(sides) + layers - owner)
+    for n in range(2, len(stages)):
+        meet(n)
+        if n + 1 < len(stages):
+            announce(n + 1)
+    for j in range(3):
+        to_far_layer(j).wait_recv()
+        for d in range(1, layers):
+            to_layer(j, d).start()
     for h in halos:
         h.start()
 
-    shared_hbm = [sgate_hbm, sup_hbm, sdown_hbm]
-
-    def held_eighth(j, i):
-        n = shared_hbm[j].shape[0] // eighths
-        if j < 2:
-            return [sgate, sup][j].at[1, pl.ds(pl.multiple_of(i * n, n), n)]
-        return sdown.at[pl.ds(pl.multiple_of(units + i * n, n), n)]
-
-    def held_layer(j, at_layer):
-        n = shared_hbm[j].shape[0] // (eighths * layers)
-        first = pl.multiple_of((eighth * layers + at_layer) * n, n)
-        if j < 2:
-            return [sgate, sup][j].at[1, pl.ds(first, n)]
-        return sdown.at[pl.ds(pl.multiple_of(units + first, n), n)]
-
-    def to_far_layer(j):
-        n = shared_hbm[j].shape[0] // (eighths * layers)
-        first = pl.multiple_of((eighth * layers + layer) * n, n)
-        return remote(
-            shared_hbm[j].at[pl.ds(first, n)],
-            held_layer(j, layer),
-            eighth_send.at[j],
-            layer_recv.at[3 * layer + j],
-            ep,
-            far,
-        )
-
-    def layer_device(d):
-        return 2 * ((z - layer + lax.rem(layer + d, layers)) * rings + y) + core
-
-    def to_layer(j, d):
-        return remote(
-            held_layer(j, layer),
-            held_layer(j, layer),
-            layer_send.at[3 * d + j],
-            layer_recv.at[3 * layer + j],
-            layer_device(d),
-            x,
-        )
-
-    def from_layer(j, d):
-        source = lax.rem(layer + d, layers)
-        return remote(
-            held_layer(j, source),
-            held_layer(j, source),
-            layer_send.at[3 * d + j],
-            layer_recv.at[3 * source + j],
-            layer_device(d),
-            x,
-        )
-
-    tiles = width // tile // 2
-
-    def round_ring(j, d):
-        return remote(
-            held_eighth(j, eighth),
-            held_eighth(j, eighth),
-            ring_send.at[3 * d + j],
-            eighth_recv.at[3 * eighth + j],
-            2 * (chip - y + lax.rem(y + d, rings)) + core,
-            x,
-        )
-
-    def opposite(j):
-        d = 1 if j == 1 else rings - 1
-        i = 2 * lax.rem(y + d, rings) + core
-        return remote(
-            held_eighth(j, i),
-            held_eighth(j, i),
-            ring_send.at[j],
-            eighth_recv.at[3 * i + j],
-            2 * (chip - y + lax.rem(y + rings - d, rings)) + core,
-            x,
-        )
-
-    def from_ring(j, d):
-        i = 2 * lax.rem(y + d, rings) + core
-        return remote(
-            held_eighth(j, i),
-            held_eighth(j, i),
-            pass_send.at[3 * d + j],
-            eighth_recv.at[3 * i + j],
-            twin,
-            x,
-        )
-
-    def from_twin(j, d):
-        i = 2 * lax.rem(y + d, rings) + 1 - core
-        return remote(
-            held_eighth(j, i),
-            held_eighth(j, i),
-            pass_send.at[3 * d + j],
-            eighth_recv.at[3 * i + j],
-            twin,
-            x,
-        )
-
-    for j in range(3):
-        to_far_layer(j).start()
-
     @pl.loop(0, experts)
     def _(i):
-        e = spread_order(i)
-
-        @pl.when(e != own_index)
+
+        @pl.when(i + 1 - owner > 0)
         def _():
-            send_out(e).start()
-
-    @pl.when(owner == 1)
-    def _():
-        for j in range(PIECES):
-            to_near(j).start()
-        for j in range(PIECES):
-            to_twin(0, j).start()
+            send_out(i).start()
 
     @pl.when(owner == 0)
     def _():
-        for j in range(PIECES):
+        for j in range(1, PIECES):
             to_far(j).start()
 
     def relay(j):
@@ -410,7 +481,7 @@
 
     @pl.when(owner == 1)
     def _():
-        landed[ep] = outgoing[ep]
+        landed[0] = outgoing[ep]
 
     share = [weights[k : k + 1, at] for k in range(2)]
     spread = jnp.where(slot_ids == place[0], share[0], 0.0) + jnp.where(
@@ -452,10 +523,6 @@
         part = dot(gated[...], outw[:, cols]).astype(bf16)
         mixer_part[lax.div(i, tiles), :, :, some] = part.reshape(4, block, tile)
 
-    for j in range(3):
-        to_far_layer(j).wait_recv()
-        for d in range(1, layers):
-            to_layer(j, d).start()
     pass_near(0)
     pass_near(1)
     relay(0)
@@ -486,69 +553,53 @@
 
     @pl.when(owner == 1)
     def _():
-        some = landed.at[pl.ds(0, experts - 1)]
+        some = landed.at[pl.ds(0, half_experts - 1)]
         remote(some, some, out_send.at[0], out_recv.at[0], twin, x).wait_recv()
+        for j in range(PIECES):
+            keep_own(j).wait()
 
     @pl.when(owner == 0)
     def _():
-        remote(landed, landed, out_send.at[0], out_recv.at[0], twin, x).wait_recv()
-
-    half = slots // 2
-    half_experts = experts // 2
-
-    @pl.loop(0, width // tile)
-    def _(i):
-        cols = pl.ds(pl.multiple_of(i * tile, tile), tile)
-        rows[:, cols] = landed[:, :, cols].reshape(slots, tile)
-
-    def gate_up(k):
-        cols = pl.ds(pl.multiple_of(k * units, units), units)
-
-        @pl.loop(0, 2)
-        def _(m):
-            r = pl.ds(pl.multiple_of(m * half, half), half)
-            g = dot(rows[r, :], wgate[k])
-            u = dot(rows[r, :], wup[k])
-            act[r, cols] = (g / (1.0 + jnp.exp(-g)) * u).astype(bf16)
-
+        some = landed.at[pl.ds(0, half_experts)]
+        remote(some, some, out_send.at[0], out_recv.at[0], twin, x).wait_recv()
+
+    def take_rows(m):
+        @pl.loop(0, width // tile)
+        def _(i):
+            cols = pl.ds(pl.multiple_of(i * tile, tile), tile)
+            rows[m * half : (m + 1) * half, cols] = landed[
+                m * half_experts : (m + 1) * half_experts, :, cols
+            ].reshape(half, tile)
+
+    def gate_up(k, m):
+        r = pl.ds(m * half, half)
+        g = dot(rows[r, :], wgate[k])
+        u = dot(rows[r, :], wup[k])
+        act[r, k * units : (k + 1) * units] = (g / (1.0 + jnp.exp(-g)) * u).astype(bf16)
+
+    take_rows(0)
     for k in range(3):
 
         @pl.when(owner == 0)
         def _():
-            for j in range(2):
+            for j in range(PIECES):
                 to_twin(k, j).wait_recv()
 
-        if k == 0:
-
-            @pl.when(owner == 1)
-            def _():
-                for j in range(2):
-                    keep_own(j).wait()
-
-        gate_up(k)
-        if k == 1:
-            passed(1)
-
-    @pl.when(owner == 0)
-    def _():
-        for k in range(3):
-            for j in range(2, PIECES):
-                to_twin(k, j).wait_recv()
-
-    @pl.when(owner == 1)
-    def _():
-        for j in range(2, PIECES):
-            keep_own(j).wait()
-
-    @pl.loop(0, width // tile)
-    def _(i):
-        cols = pl.ds(pl.multiple_of(i * tile, tile), tile)
-        for m in range(2):
-            r = pl.ds(m * half, half)
-            total = dot(act[r, 0:units], wdown[0, :, cols])
-            for k in range(1, 3):
-                total = total + dot(act[r, k * units : (k + 1) * units], wdown[k, :, cols])
-            total_down[r, cols] = total
+        gate_up(k, 0)
+    passed(1)
+
+    for i in range(width // tile):
+        cols = pl.ds(i * tile, tile)
+        total = dot(act[0:half, 0:units], wdown[0, :, cols])
+        for k in range(1, 3):
+            total = total + dot(act[0:half, k * units : (k + 1) * units], wdown[k, :, cols])
+        total_down[:, cols] = total
+
+    some = landed.at[pl.ds(half_experts, half_experts)]
+    remote(some, some, out_send.at[0], out_recv.at[1], twin, x).wait_recv()
+    take_rows(1)
+    for k in range(3):
+        gate_up(k, 1)
 
     for j in range(3):
         for d in sides:
@@ -564,7 +615,8 @@
         def _():
             to_twin(3, j).wait_recv()
 
-    gate_up(3)
+    gate_up(3, 0)
+    gate_up(3, 1)
 
     group_copy = remote(
         group.at[own_rows], group.at[near_rows], group_send.at[0], group_recv.at[0], ep, near
@@ -609,36 +661,45 @@
     for b in (1, 0):
         first_copy(0, b).start()
 
-    def send_back(s):
-        return remote(
-            results.at[s], returned.at[mine], back_send.at[0], back_recv.at[0], s, plane
+    def send_back(i):
+        return remote(
+            results.at[i],
+            returned.at[mine],
+            back_send.at[0],
+            back_recv.at[0],
+            source_order(i),
+            plane,
         )
 
     def down(m):
         r = pl.ds(m * half, half)
-        e = pl.ds(m * half_experts, half_experts)
         for i in range(width // tile):
             cols = pl.ds(i * tile, tile)
-            total = total_down[r, cols] + dot(act[r, 3 * units : 4 * units], wdown[3, :, cols])
-            results[e, :, cols] = total.reshape(half_experts, capacity, tile).astype(bf16)
+            total = dot(act[r, 3 * units : 4 * units], wdown[3, :, cols])
+            if m == 0:
+                total = total + total_down[:, cols]
+            else:
+                for k in range(3):
+                    total = total + dot(act[r, k * units : (k + 1) * units], wdown[k, :, cols])
+            results[m * half_experts : (m + 1) * half_experts, :, cols] = total.reshape(
+                half_experts, capacity, tile
+            ).astype(bf16)
+
+        @pl.loop(m * half_experts, (m + 1) * half_experts)
+        def _(i):
+            @pl.when(i + 1 - owner > 0)
+            def _():
+                send_back(i).start()
 
     down(0)
     down(1)
 
-    @pl.loop(0, experts)
-    def _(i):
-        s = spread_order(i)
-
-        @pl.when(s != own_index)
-        def _():
-            send_back(s).start()
-
     for b in (1, 0):
         first_copy(1, b).start()
 
     @pl.when(owner == 1)
     def _():
-        returned[ep] = results[ep]
+        returned[ep] = results[0]
 
     for d in range(2, rings - 1):
         for j in range(3):
@@ -802,7 +863,7 @@
     capacity = 2 * block * routes.shape[1] // experts
     slots = experts * capacity
     rings = 4 if experts % 32 == 0 else 2
-    layers = min(4, experts // (2 * rings))
+    layers = min(2, experts // (2 * rings))
     tile = min(256, width)
     vmem = pl.BlockSpec(memory_space=pltpu.VMEM)
     hbm = pl.BlockSpec(memory_space=pl.ANY)
@@ -845,7 +906,7 @@
             space(slots, block),
             space(block, slots),
             space(block, slots),
-            pltpu.VMEM((slots, width), f32),
+            pltpu.VMEM((slots // 2, width), f32),
             space(2, 4, block, width // 2),
             pltpu.VMEM((block, width), f32),
             space(block, width),
@@ -859,7 +920,7 @@
             dma((1,)),
             dma((1,)),
             dma((1,)),
-            dma((1,)),
+            dma((2,)),
             dma((PIECES,)),
             dma((PIECES,)),
             dma((2 * PIECES,)),
@@ -879,6 +940,7 @@
             dma((6 * rings,)),
             dma((1,)),
             dma((1,)),
+            pltpu.SemaphoreType.REGULAR((8,)),
         ],
         compiler_params=pltpu.CompilerParams(
             collective_id=0, has_side_effects=True, vmem_limit_bytes=60 * 1024 * 1024

time: 142 us -> 136 us (0.958)
  Pallas kernels: 141 us -> 135 us
    pallas_call x1, Pallas kernels: 139 us -> 133 us  [per_device(): pl.pallas_call(functools.partial(kernel, experts, capacity, rings, layers...]
where the time goes in v6:
time: 136 us
  Pallas kernels  135 us (99%)
    pallas_call x1, Pallas kernels, per_device(): pl.pallas_call(functools.partial(kernel, experts, capacity, rings, layers...  133 us

profile of v6, /device:TPU:1, one launch (start us, length us, event | category | flops | bytes accessed | tf_op | source)
XLA Modules:
  0.0 136.1 jit_solution(16572266953432923988)
XLA Ops:
  0.6 133.4 %whole.1 = (bf16[128,2048]{1,0:T(8,128)(2,1)}, bf16[128,2048]{1,0:T(8,128)(2,1)}) custom-call(bf16[512,512]{1,0:T(8,128)(2,1)} %outer_hbm.1, bf16[512,512]{1,0:T(8,128)(2,1)} %inner_hbm.1, bf16[512,512]{1,0:T(8,128)(2,1)} %values_hbm.1, bf16[3,512]{1,0:T(4,128)(2,1)} %taps.1, bf16[512,2048]{1,0:T(8,128)(2,1)} %outw_hbm.1, bf16[128,2048]{1,0:T(8,128)(2,1)} %moe_hbm.1, ...), custom_call_target="tpu_custom_call" | custom-call | tf_op jit(solution)/shard_map/whole/pallas_call | solution.py:876
  134.1 2.0 %leave.1 = (bf16[128,2048]{1,0:T(8,128)(2,1)}, bf16[128,2048]{1,0:T(8,128)(2,1)}) custom-call(bf16[128,2048]{1,0:T(8,128)(2,1)} %get-tuple-element.4.mixer_in, bf16[128,2048]{1,0:T(8,128)(2,1)} %get-tuple-element.5.expert_in), custom_call_target="tpu_custom_call" | custom-call | tf_op jit(solution)/shard_map/leave/pallas_call | solution.py:965

commit v7 on v6

--- a/solution.py
+++ b/solution.py
@@ -12,7 +12,7 @@
 bf16 = jnp.bfloat16
 f32 = jnp.float32
 HALO = 16
-PIECES = 6
+PIECES = 7
 
 
 def remote(src, dst, send_sem, recv_sem, ep, tp):
@@ -39,18 +39,18 @@
     outer_hbm,
     inner_hbm,
     values_hbm,
-    taps,
+    taps_hbm,
     outw_hbm,
     moe_hbm,
-    gain,
+    gain_hbm,
     gate_hbm,
     up_hbm,
     down_hbm,
     sgate_hbm,
     sup_hbm,
     sdown_hbm,
-    routes,
-    weights,
+    routes_hbm,
+    weights_hbm,
     mixer_out,
     expert_out,
     moe,
@@ -114,6 +114,11 @@
     back_send,
     back_recv,
     met,
+    taps,
+    gain,
+    routes,
+    weights,
+    small_sem,
 ):
     ep, x = lax.axis_index("ep"), lax.axis_index("tp")
     core, chip = lax.rem(ep, 2), lax.div(ep, 2)
@@ -147,18 +152,23 @@
     ]
     loads = [pltpu.make_async_copy(s, d, load_sem.at[i]) for i, (s, d) in enumerate(loads)]
     loads[0].start()
-
-    quarter = units // 4
+    small = [(routes_hbm, routes), (gain_hbm, gain), (weights_hbm, weights), (taps_hbm, taps)]
+    small = [pltpu.make_async_copy(s, d, small_sem.at[i]) for i, (s, d) in enumerate(small)]
+
+    cuts = [units * c // 8 for c in (0, 2, 4, 6, 7, 8)]
+
+    def down_rows(j):
+        return pl.ds(cuts[j - 2], cuts[j - 1] - cuts[j - 2])
 
     def own_piece(j):
         if j < 2:
             return [gate_hbm, up_hbm][j].at[0]
-        return down_hbm.at[0, pl.ds((j - 2) * quarter, quarter)]
+        return down_hbm.at[0, down_rows(j)]
 
     def held_piece(k, j):
         if j < 2:
             return [wgate, wup][j].at[k]
-        return wdown.at[k, pl.ds((j - 2) * quarter, quarter)]
+        return wdown.at[k, down_rows(j)]
 
     def weight_copy(src, k, j, send, device, tp):
         return remote(src, held_piece(k, j), send, weight_recv.at[PIECES * k + j], device, tp)
@@ -204,7 +214,8 @@
     def above(d):
         return lax.div(2 * deep - 1 - z - d, deep)
 
-    for d in sides:
+    ring = list(range(1, rings))
+    for d in ring:
         greet(along_y(d), x)
 
     def tell_z(d, tell):
@@ -223,7 +234,7 @@
         for j in range(PIECES):
             keep_own(j).start()
 
-    for c in loads[1:]:
+    for c in small + loads[1:]:
         c.start()
 
     after = lax.rem(ep + 1, experts)
@@ -330,7 +341,7 @@
             x,
         )
 
-    pl.semaphore_wait(barrier, 3 + len(sides) + below(1) + above(1))
+    pl.semaphore_wait(barrier, 3 + len(ring) + below(1) + above(1))
     for j in range(3):
         to_far_layer(j).start()
 
@@ -345,7 +356,7 @@
     def _():
         to_far(0).start()
 
-    stages = [None] + [sides] * (2 if rings > 2 else 1)
+    stages = [None, ring]
     stages += [d for d in (1, 2, 4) if d < deep]
 
     def announce(n):
@@ -373,6 +384,7 @@
 
     announce(0)
 
+    small[0].wait()
     at = pl.ds(pl.multiple_of(x * block, block), block)
     chosen = [routes[k : k + 1, at].astype(f32) for k in range(2)]
     expert_ids = lax.broadcasted_iota(jnp.int32, (experts, block), 0).astype(f32)
@@ -394,6 +406,7 @@
     announce(1)
 
     loads[0].wait()
+    small[1].wait()
     scale = gain[...].reshape(1, width).astype(f32)
     step = min(16, block)
 
@@ -483,6 +496,7 @@
     def _():
         landed[0] = outgoing[ep]
 
+    small[2].wait()
     share = [weights[k : k + 1, at] for k in range(2)]
     spread = jnp.where(slot_ids == place[0], share[0], 0.0) + jnp.where(
         slot_ids == place[1], share[1], 0.0
@@ -492,7 +506,7 @@
     spread_hi[...] = high
     spread_lo[...] = (spread - high.astype(f32)).astype(bf16)
 
-    for c in loads[1:4]:
+    for c in loads[1:4] + small[3:]:
         c.wait()
     for h in halos:
         h.wait_recv()
@@ -539,8 +553,8 @@
         for d in sides:
             round_ring(j, d).start()
         from_ring(j, 0).start()
-    relay(4)
-    relay(5)
+    for j in range(4, PIECES):
+        relay(j)
 
     def passed(j):
         @pl.when(owner == 1)
@@ -821,21 +835,14 @@
         remote(results, results, back_send.at[0], back_recv.at[0], twin, x).wait_send()
 
 
-def leave(mixer_in, expert_in, mixer_out, expert_out, mixer, expert, in_sem, out_sem):
-    ins = [
-        pltpu.make_async_copy(mixer_in, mixer, in_sem.at[0]),
-        pltpu.make_async_copy(expert_in, expert, in_sem.at[1]),
+def leave(mixer, expert, mixer_out, expert_out, sem):
+    copies = [
+        pltpu.make_async_copy(mixer, mixer_out, sem.at[0]),
+        pltpu.make_async_copy(expert, expert_out, sem.at[1]),
     ]
-    outs = [
-        pltpu.make_async_copy(mixer, mixer_out, out_sem.at[0]),
-        pltpu.make_async_copy(expert, expert_out, out_sem.at[1]),
-    ]
-    for c in ins:
+    for c in copies:
         c.start()
-    for i, o in zip(ins, outs):
-        i.wait()
-        o.start()
-    for c in outs:
+    for c in copies:
         c.wait()
 
 
@@ -876,8 +883,8 @@
     outs = pl.pallas_call(
         functools.partial(kernel, experts, capacity, rings, layers, tile),
         name="whole",
-        out_shape=(out, out),
-        in_specs=[hbm, hbm, hbm, vmem, hbm, hbm, vmem] + [hbm] * 6 + [vmem, vmem],
+        out_shape=(pltpu.VMEM(out.shape, bf16), pltpu.VMEM(out.shape, bf16)),
+        in_specs=[hbm] * 15,
         out_specs=(vmem, vmem),
         scratch_shapes=[
             space(block, width),
@@ -941,6 +948,11 @@
             dma((1,)),
             dma((1,)),
             pltpu.SemaphoreType.REGULAR((8,)),
+            space(*conv_taps.shape),
+            space(width),
+            pltpu.VMEM(routes.shape[::-1], jnp.int32),
+            pltpu.VMEM(route_weight.shape[::-1], f32),
+            dma((4,)),
         ],
         compiler_params=pltpu.CompilerParams(
             collective_id=0, has_side_effects=True, vmem_limit_bytes=60 * 1024 * 1024
@@ -966,10 +978,10 @@
         leave,
         name="leave",
         out_shape=(out, out),
-        in_specs=[hbm, hbm],
+        in_specs=[vmem, vmem],
         out_specs=(hbm, hbm),
-        scratch_shapes=[space(block, width), space(block, width), dma((2,)), dma((2,))],
-    )(*outs)
+        scratch_shapes=[dma((2,))],
+    )(*[pltpu.with_memory_space_constraint(o, pltpu.VMEM) for o in outs])
 
 
 def solution(mesh):

time: 136 us -> 134 us (0.985)
  Pallas kernels: 135 us -> 133 us
where the time goes in v7:
time: 134 us
  Pallas kernels  133 us (99%)
    pallas_call x1, Pallas kernels, per_device(): pl.pallas_call(functools.partial(kernel, experts, capacity, rings, layers...  132 us

profile of v7, /device:TPU:1, one launch (start us, length us, event | category | flops | bytes accessed | tf_op | source)
XLA Modules:
  0.0 134.0 jit_solution(16576977594626117706)
XLA Ops:
  0.6 132.4 %whole.1 = (bf16[128,2048]{1,0:T(8,128)(2,1)S(1)}, bf16[128,2048]{1,0:T(8,128)(2,1)S(1)}) custom-call(bf16[512,512]{1,0:T(8,128)(2,1)} %outer_hbm.1, bf16[512,512]{1,0:T(8,128)(2,1)} %inner_hbm.1, bf16[512,512]{1,0:T(8,128)(2,1)} %values_hbm.1, bf16[3,512]{1,0:T(4,128)(2,1)} %taps_hbm.1, bf16[512,2048]{1,0:T(8,128)(2,1)} %outw_hbm.1, ...), custom_call_target="tpu_custom_call" | custom-call | tf_op jit(solution)/shard_map/whole/pallas_call | solution.py:883
  133.0 1.0 leave.1

commit v8 on v7

--- a/solution.py
+++ b/solution.py
@@ -467,9 +467,8 @@
     for h in halos:
         h.start()
 
-    @pl.loop(0, experts)
+    @pl.loop(0, experts, unroll=8)
     def _(i):
-
         @pl.when(i + 1 - owner > 0)
         def _():
             send_out(i).start()
@@ -699,7 +698,7 @@
                 half_experts, capacity, tile
             ).astype(bf16)
 
-        @pl.loop(m * half_experts, (m + 1) * half_experts)
+        @pl.loop(m * half_experts, (m + 1) * half_experts, unroll=8)
         def _(i):
             @pl.when(i + 1 - owner > 0)
             def _():

time: 134 us -> 134 us (level)
  no operation moved by 1% of the time
where the time goes in v8:
time: 134 us
  Pallas kernels  133 us (99%)
    pallas_call x1, Pallas kernels, per_device(): pl.pallas_call(functools.partial(kernel, experts, capacity, rings, layers...  132 us

profile of v8, /device:TPU:1, one launch (start us, length us, event | category | flops | bytes accessed | tf_op | source)
XLA Modules:
  0.0 134.0 jit_solution(9977624502786885958)
XLA Ops:
  0.6 132.4 %whole.1 = (bf16[128,2048]{1,0:T(8,128)(2,1)S(1)}, bf16[128,2048]{1,0:T(8,128)(2,1)S(1)}) custom-call(bf16[512,512]{1,0:T(8,128)(2,1)} %outer_hbm.1, bf16[512,512]{1,0:T(8,128)(2,1)} %inner_hbm.1, bf16[512,512]{1,0:T(8,128)(2,1)} %values_hbm.1, bf16[3,512]{1,0:T(4,128)(2,1)} %taps_hbm.1, bf16[512,2048]{1,0:T(8,128)(2,1)} %outw_hbm.1, ...), custom_call_target="tpu_custom_call" | custom-call | tf_op jit(solution)/shard_map/whole/pallas_call | solution.py:882
  133.0 1.0 leave.1
